TPU v7x, 32 devices: a whole 2x2x4 slice. The times are simulated.
32 devices in a mesh: sp: 16 (over z, y, x), tp: 2 (over core).
Axes of the slice: x: 2, y: 2, z: 4, core: 2. Of those that a mesh axis runs over, the one named last changes fastest.
Arguments:
- stream_in: bfloat16 [4096, 2048], P('sp'), may hold values from -6 to 6
- norm_gain: float32 [2, 2048], replicated, may hold values from 0.1 to 1.9
- value_weight: bfloat16 [2, 2048, 2048], P(None, 'sp', 'tp'), may hold values from -0.125 to 0.125
- gate_weight: bfloat16 [2, 2048, 2048], P(None, 'sp', 'tp'), may hold values from -0.125 to 0.125
- conv_taps: float32 [2, 31, 2048], P(None, None, 'tp'), may hold values from -5 to 5
- channel_gain: float32 [2, 2048], P(None, 'tp'), may hold values from 0.1 to 1.9
- out_weight: bfloat16 [2, 2048, 2048], P(None, 'tp', 'sp'), may hold values from -0.125 to 0.125
Outputs:
- stream_out: bfloat16 [4096, 2048], P('sp')
All inputs are finite; a program needn't handle non-finite values.
Results may differ from a plain program's by a relative error of at most 0.015.
Values may be sent and summed in bfloat16 or wider, within the bound.
A program may use at most 64 MiB of HBM per device.

v0:
```python
import functools

import jax
import jax.numpy as jnp
from jax import lax
from jax.experimental import pallas as pl
from jax.experimental.pallas import tpu as pltpu
from jax.sharding import PartitionSpec as P

epsilon = 1e-05
MESH = pl.DeviceIdType.MESH
F32 = jnp.float32
BF16 = jnp.bfloat16
PAD = 32
EARLY, EARLY_LAST = 3, 2
SPLIT = 1


def kernel(n, layers, taps_n, stream_in, gain, vw, gw, taps, cgain, ow, out,
           wv, wg, wo, nrm, gat, hsend, hrecv, fil, ssend, srecv, act,
           dsend, drecv, xsend, xrecv, strm, keep,
           loc_sem, wx_send, wx_recv, ring_send, ring_recv, msg_send, msg_recv):
    ring = n // 2
    s = lax.axis_index("sp")
    c = lax.axis_index("tp")
    o, i = s // 2, s % 2
    toks, width = stream_in.shape
    group = 2 * toks
    rows, cols = vw.shape[1], vw.shape[2]
    ch = cols // 2
    half = width // 2

    def place(outer):
        z, y = outer // 2, outer % 2
        return (1 - y) * z + y * (ring - 1 - z)

    def outer_at(pos):
        h = pos // (ring // 2)
        return 2 * ((1 - h) * pos + h * (ring - 1 - pos)) + h

    p = place(o)
    nxt = outer_at((p + 1) % ring) * 2 + i
    prv = outer_at((p + ring - 1) % ring) * 2 + i
    mate = o * 2 + 1 - i
    up = ((o + 1) % ring) * 2 + i
    down = ((o + ring - 1) % ring) * 2 + i
    x_dev, d_dev, xd_dev = (mate, c), (s, 1 - c), (mate, 1 - c)

    barrier = pltpu.get_barrier_semaphore()
    everyone = [x_dev, d_dev, xd_dev, (nxt, c), (prv, c), (up, c), (down, c)]
    for dev in everyone:
        pl.semaphore_signal(barrier, inc=1, device_id=dev, device_id_type=MESH)
    pl.semaphore_wait(barrier, len(everyone))

    def al(v, m):
        return pl.multiple_of(v, m)

    my_rows = pl.ds(al(s * rows, rows), rows)
    my_cols = pl.ds(al(i * ch, ch), ch)
    mate_cols = pl.ds(al((1 - i) * ch, ch), ch)

    def weight_views(l, kind):
        if kind == 0:
            return vw.at[l, :, my_cols], vw.at[l, :, mate_cols], wv.at[l, my_rows, :]
        if kind == 1:
            return gw.at[l, :, my_cols], gw.at[l, :, mate_cols], wg.at[l, my_rows, :]
        return ow.at[l, my_cols, :], ow.at[l, mate_cols, :], wo.at[l, :, my_rows]

    local, crossed = {}, {}

    def start_local(l, kind):
        src, _, dst = weight_views(l, kind)
        local[l, kind] = pltpu.make_async_copy(src, dst, loc_sem.at[l * 3 + kind])
        local[l, kind].start()

    def start_cross(l, kind):
        _, src, dst = weight_views(l, kind)
        crossed[l, kind] = pltpu.make_async_remote_copy(
            src, dst, wx_send.at[l * 3 + kind], wx_recv.at[l * 3 + kind],
            device_id=x_dev, device_id_type=MESH)
        crossed[l, kind].start()

    pending = {}

    def block_cols(pos, d):
        return pl.ds(al((outer_at(pos) * 2 + d) * rows, rows), rows)

    def chunk(l, grp, d, q, pos):
        if grp == 0:
            block = outer_at(pos) * 2 + (i + q // SPLIT) % 2
            w, size = (wv if d == 0 else wg), rows // SPLIT
            return w.at[l, pl.ds(al(block * rows + q % SPLIT * size, size), size), :]
        size = ch // 2 // SPLIT
        return wo.at[l, pl.ds(q * size, size), block_cols(pos, d)]

    def own_ready(l, grp, q):
        if grp == 0 and q % SPLIT == 0:
            for kind in (0, 1):
                (crossed if q else local)[l, kind].wait()
        if grp == 1 and q == 0:
            local[l, 2].wait()
            crossed[l, 2].wait()

    def pump(l, grp, t):
        for q in range(2 * SPLIT):
            if t == 0:
                own_ready(l, grp, q)
            for d in range(2):
                k = (l * 2 + grp) * 2 + d
                if t > 0:
                    pending[k, q].wait()
                if t < ring - 1:
                    pos = (p + ring - t) % ring if d == 0 else (p + t) % ring
                    ref = chunk(l, grp, d, q, pos)
                    pending[k, q] = pltpu.make_async_remote_copy(
                        ref, ref, ring_send.at[k, q], ring_recv.at[k, q, t],
                        device_id=(nxt if d == 0 else prv, c), device_id_type=MESH)
                    pending[k, q].start()

    queue = []
    for l in range(layers):
        main = [(l, 0, t) for t in range(1 if l else 0, ring)]
        side = [(l, 1, t) for t in range(ring)]
        early = min(EARLY if l + 1 < layers else EARLY_LAST, ring)
        queue += main[:len(main) - early]
        for t in range(early):
            queue += [main[len(main) - early + t], side[t]]
        rest = side[early:]
        queue += rest[:len(rest) // 2]
        if l + 1 < layers:
            queue.append((l + 1, 0, 0))
        queue += rest[len(rest) // 2:]
    done = []

    def pumps(count):
        for _ in range(count):
            if queue:
                item = queue.pop(0)
                pump(*item)
                done.append(item)

    def ensure(l, grp, t):
        while (l, grp, t) not in done:
            pumps(1)

    def message(slot, src, dst, dev):
        m = pltpu.make_async_remote_copy(src, dst, msg_send.at[slot], msg_recv.at[slot],
                                         device_id=dev, device_id_type=MESH)
        m.start()
        return m

    for l in range(layers):
        for kind in range(3):
            start_local(l, kind)
    start_cross(0, 0)
    start_cross(0, 1)

    own_tok = al(i * toks, toks)
    mate_tok = al((1 - i) * toks, toks)
    own_half = pl.ds(al(c * half, half), half)
    tile = 128 if toks % 128 == 0 else toks
    per_layer = 6 + ring * 3

    for l in range(layers):
        base = l * per_layer
        source = stream_in if l == 0 else strm.at[l - 1]

        def norm_step(r, _):
            at = al(r * 64, 64)
            wide = source[pl.ds(at, 64), :].astype(F32)
            scale = lax.rsqrt(jnp.mean(wide * wide, axis=1, keepdims=True) + epsilon)
            nrm[l, pl.ds(al(own_tok + at, 64), 64), :] = (wide * scale * gain[l:l + 1, :]).astype(BF16)
            return 0

        lax.fori_loop(0, toks // 64, norm_step, 0)
        spot = nrm.at[l, pl.ds(own_tok, toks), own_half]
        got = nrm.at[l, pl.ds(mate_tok, toks), own_half]
        gather = message(base + 0, spot, spot, x_dev)
        if l == 0:
            start_cross(0, 2)
            for ll in range(1, layers):
                for kind in range(3):
                    start_cross(ll, kind)
            pumps(3)
        else:
            pumps(4)
        gather.wait()
        relay = message(base + 1, got, got, d_dev)
        ensure(l, 0, ring - 1)
        relay.wait()

        def gate_step(r, _):
            at = al(r * tile, tile)
            x = nrm[l, pl.ds(at, tile), :]
            value = jnp.dot(x, wv[l], preferred_element_type=F32)
            gate = jnp.dot(x, wg[l], preferred_element_type=F32)
            gated = (value * jax.nn.sigmoid(gate)).astype(BF16)
            gat[pl.ds(al(PAD + at, 32), tile), :] = gated.astype(F32)
            return 0

        lax.fori_loop(0, group // tile, gate_step, 0)
        hsend[l] = gat[group:group + PAD, :].astype(BF16)
        halo = message(base + 2, hsend.at[l], hrecv.at[l], (up, c))
        pumps(1)
        halo.wait()
        first = (o > 0).astype(F32)
        gat[0:PAD, :] = hrecv[l].astype(F32) * first

        lead = PAD - (taps_n - 1)
        step_rows = 64
        lanes = 128

        def conv_step(r, _):
            at = al(r * step_rows, step_rows)
            for lane in range(ch // lanes):
                cut = slice(lane * lanes, (lane + 1) * lanes)
                total = jnp.zeros((step_rows, lanes), F32)
                block = gat[pl.ds(at, step_rows + PAD), cut]
                for b in range(8):
                    moved = block if b == 0 else pltpu.roll(block, step_rows + PAD - b, 0)
                    for a in range(PAD // 8 + 1):
                        tap = 8 * a + b - lead
                        if 0 <= tap < taps_n:
                            total = total + taps[l, tap:tap + 1, cut] * moved[8 * a:8 * a + step_rows]
                fil[pl.ds(at, step_rows), cut] = total
            return 0

        parts = 2
        per = group // step_rows // parts
        for part in range(parts):
            lax.fori_loop(part * per, (part + 1) * per, conv_step, 0)
            pumps(1)

        wide = fil[...]
        first_sum = jnp.sum(wide, axis=1, keepdims=True)
        second_sum = jnp.sum(wide * wide, axis=1, keepdims=True)
        lane_id = lax.broadcasted_iota(jnp.int32, (group, lanes), 1)
        stat = jnp.where(lane_id == 0, first_sum, jnp.where(lane_id == 1, second_sum, 0.0))
        ssend[l] = jnp.transpose(stat)[0:8, :]
        sums = [message(base + 3 + k, ssend.at[l], srecv.at[l, k], dev)
                for k, dev in enumerate((x_dev, d_dev, xd_dev))]
        pumps(1)
        for m in sums:
            m.wait()
        whole = ssend[l] + srecv[l, 0] + srecv[l, 1] + srecv[l, 2]
        stat = jnp.transpose(jnp.concatenate([whole] + [jnp.zeros((lanes - 8, group), F32)], axis=0))
        mean_value = stat[:, 0:1] / width
        variance = stat[:, 1:2] / width - mean_value * mean_value
        act[...] = jax.nn.silu((fil[...] - mean_value) * lax.rsqrt(variance + epsilon)
                               * cgain[l:l + 1, pl.ds(al(i * ch, ch), ch)]).astype(BF16)

        slot = base + 6
        own_rows, mate_rows = pl.ds(own_tok, toks), pl.ds(mate_tok, toks)
        swaps, scatters, lasts = [], [], []

        def own_block(u):
            return block_cols((p + ring + (2 * c - 1) * u) % ring, c)

        def stage_swap(u):
            columns = block_cols((p + ring + (1 - 2 * c) * u) % ring, 1 - c)
            dsend[l, u] = jnp.dot(act[...], wo[l, :, columns], preferred_element_type=F32).astype(BF16)
            swaps.append(message(slot + u, dsend.at[l, u], drecv.at[l, u], d_dev))

        def stage_scatter(u):
            weights = wo[l, :, own_block(u)]
            away = jnp.dot(act[mate_rows, :], weights, preferred_element_type=F32)
            mine = jnp.dot(act[own_rows, :], weights, preferred_element_type=F32)
            swaps[u].wait()
            xsend[l, u] = (away + drecv[l, u, mate_rows, :].astype(F32)).astype(BF16)
            scatters.append(message(slot + ring + u, xsend.at[l, u], xrecv.at[l, u], x_dev))
            keep[u] = (mine + drecv[l, u, own_rows, :].astype(F32)
                       + source[:, own_block(u)].astype(F32))

        def stage_last(u):
            scatters[u].wait()
            strm[l, :, own_block(u)] = (keep[u] + xrecv[l, u].astype(F32)).astype(BF16)
            piece = strm.at[l, :, own_block(u)]
            lasts.append(message(slot + 2 * ring + u, piece, piece, d_dev))

        lag = 2
        for u in range(ring + 1 + lag):
            if u < ring:
                ensure(l, 1, u)
                stage_swap(u)
            if 1 <= u <= ring:
                stage_scatter(u - 1)
            if u % 3 == 1:
                pumps(1 if l + 1 < layers else 0)
            if u >= 1 + lag:
                stage_last(u - 1 - lag)
        for m in lasts:
            m.wait()

    out[...] = strm[layers - 1]


def fused(n, layers):
    def body(stream_in, norm_gain, value_weight, gate_weight, conv_taps, channel_gain, out_weight):
        toks, width = stream_in.shape
        taps_n = conv_taps.shape[1]
        rows, cols = value_weight.shape[1], value_weight.shape[2]
        ch, half, group, ring = cols // 2, width // 2, 2 * toks, n // 2
        i = lax.axis_index("sp") % 2
        taps = lax.dynamic_slice_in_dim(conv_taps, i * ch, ch, axis=2)
        vmem = pl.BlockSpec(memory_space=pltpu.VMEM)
        hbm = pl.BlockSpec(memory_space=pltpu.HBM)
        msgs = layers * (6 + ring * 3)
        return pl.pallas_call(
            functools.partial(kernel, n, layers, taps_n),
            out_shape=jax.ShapeDtypeStruct((toks, width), BF16),
            in_specs=[vmem, vmem, hbm, hbm, vmem, vmem, hbm],
            out_specs=vmem,
            scratch_shapes=[
                pltpu.VMEM((layers, width, ch), BF16),
                pltpu.VMEM((layers, width, ch), BF16),
                pltpu.VMEM((layers, ch, width), BF16),
                pltpu.VMEM((layers, group, width), BF16),
                pltpu.VMEM((PAD + group, ch), F32),
                pltpu.VMEM((layers, PAD, ch), BF16),
                pltpu.VMEM((layers, PAD, ch), BF16),
                pltpu.VMEM((group, ch), F32),
                pltpu.VMEM((layers, 8, group), F32),
                pltpu.VMEM((layers, 3, 8, group), F32),
                pltpu.VMEM((group, ch), BF16),
                pltpu.VMEM((layers, ring, group, rows), BF16),
                pltpu.VMEM((layers, ring, group, rows), BF16),
                pltpu.VMEM((layers, ring, toks, rows), BF16),
                pltpu.VMEM((layers, ring, toks, rows), BF16),
                pltpu.VMEM((layers, toks, width), BF16),
                pltpu.VMEM((ring, toks, rows), F32),
                pltpu.SemaphoreType.DMA((layers * 3,)),
                pltpu.SemaphoreType.DMA((layers * 3,)),
                pltpu.SemaphoreType.DMA((layers * 3,)),
                pltpu.SemaphoreType.DMA((layers * 4, 2 * SPLIT)),
                pltpu.SemaphoreType.DMA((layers * 4, 2 * SPLIT, ring - 1)),
                pltpu.SemaphoreType.DMA((msgs,)),
                pltpu.SemaphoreType.DMA((msgs,)),
            ],
            compiler_params=pltpu.CompilerParams(
                collective_id=0, has_side_effects=True, vmem_limit_bytes=62 * 2**20),
        )(stream_in, norm_gain, value_weight, gate_weight, taps, channel_gain, out_weight)

    return body


def passed_along(value, axis, steps):
    count = lax.axis_size(axis)
    leading, last = (max(0, -steps), min(count, count - steps))
    return lax.ppermute(value, axis, [(source, source + steps) for source in range(leading, last)])


def general(stream_in, norm_gain, value_weight, gate_weight, conv_taps, channel_gain, out_weight):
    stream = stream_in
    tok_rows = stream_in.shape[0]
    width = stream_in.shape[1]
    taps_n = conv_taps.shape[1]
    local_cols = value_weight.shape[2]
    for layer in range(norm_gain.shape[0]):
        wide = stream.astype(F32)
        normed = (
            wide
            * lax.rsqrt(jnp.mean(wide * wide, axis=1, keepdims=True) + epsilon)
            * norm_gain[layer]
        ).astype(BF16)
        value = jnp.dot(normed, lax.all_gather(value_weight[layer], "sp", axis=0, tiled=True),
                        preferred_element_type=F32)
        gate = jnp.dot(normed, lax.all_gather(gate_weight[layer], "sp", axis=0, tiled=True),
                       preferred_element_type=F32)
        gated = (value * jax.nn.sigmoid(gate)).astype(BF16)
        earlier = passed_along(gated[tok_rows - (taps_n - 1):], "sp", 1)
        padded = jnp.concatenate([earlier, gated], axis=0).astype(F32)
        taps = conv_taps[layer]
        filtered = jnp.zeros((tok_rows, local_cols), F32)
        for tap in range(taps_n):
            filtered = filtered + taps[tap] * padded[tap:tap + tok_rows]
        sum_first, sum_second = lax.psum(
            (jnp.sum(filtered, axis=1), jnp.sum(filtered * filtered, axis=1)), "tp")
        mean_value = (sum_first / width)[:, None]
        variance = (sum_second / width)[:, None] - mean_value * mean_value
        activated = jax.nn.silu(
            (filtered - mean_value) * lax.rsqrt(variance + epsilon) * channel_gain[layer]
        ).astype(BF16)
        whole_out = lax.all_gather(out_weight[layer], "sp", axis=1, tiled=True)
        terms = jnp.dot(activated, whole_out, preferred_element_type=F32)
        summed = lax.psum(terms.astype(BF16), "tp").astype(F32)
        stream = (wide + summed).astype(BF16)
    return stream


def solution(mesh):
    n, tp = mesh.shape["sp"], mesh.shape["tp"]

    def body(stream_in, norm_gain, value_weight, *rest):
        rows, cols = value_weight.shape[1], value_weight.shape[2]
        pairs = tp == 2 and n % 4 == 0 and rows % 128 == 0 and cols % 1024 == 0
        fits = stream_in.shape[0] % 64 == 0 and rest[1].shape[1] <= PAD
        chosen = fused(n, norm_gain.shape[0]) if pairs and fits else general
        return chosen(stream_in, norm_gain, value_weight, *rest)

    return jax.shard_map(
        body,
        mesh=mesh,
        in_specs=(
            P("sp", None),
            P(),
            P(None, "sp", "tp"),
            P(None, "sp", "tp"),
            P(None, None, "tp"),
            P(None, "tp"),
            P(None, "tp", "sp"),
        ),
        out_specs=P("sp", None),
        check_vma=False,
    )
```

profile of v0, /device:TPU:0, one launch (start us, length us, event | category | flops | bytes accessed | tf_op | source)
XLA Modules:
  0.0 166.5 jit_solution(16971570380511530538)
XLA Ops:
  0.0 0.0 copy-start
  0.0 0.9 copy-done
  1.0 0.7 copy.9.taps
  1.6 162.5 %shard_map.73 = bf16[256,2048]{1,0:T(8,128)(2,1)} custom-call(bf16[256,2048]{1,0:T(8,128)(2,1)} %stream_in.1, f32[2,2048]{1,0:T(2,128)} %gain.1, bf16[2,128,1024]{2,1,0:T(8,128)(2,1)} %vw.1, bf16[2,128,1024]{2,1,0:T(8,128)(2,1)} %gw.1, f32[2,31,512]{2,1,0:T(8,128)} %copy.9.taps, f32[2,1024]{1,0:T(2,128)} %cgain.1, bf16[2,1024,128]{2,1,0:T(8,128)(2,1)} %ow.1), custom_call_target="tpu_custom_call" | custom-call | tf_op jit(solution)/shard_map/pallas_call | solution.py:308
  164.2 2.3 %copy.11 = bf16[256,2048]{1,0:T(8,128)(2,1)} copy(bf16[256,2048]{1,0:T(8,128)(2,1)} %shard_map.73) | data formatting | bytes 2097152
  (1 shorter events, 0.0 us)
Async XLA Ops:
  0.0 0.9 copy-start
where the time goes:
time: 167 us; the launch traced here: 166 us
  Pallas kernels  163 us (98%)
  local copies, waits for them, and re-layouts  3.94 us (2%)
    pallas_call x1, Pallas kernels, body(): pl.pallas_call(functools.partial(kernel, n, layers, taps_n), out_shape=ja...  163 us
    unnamed x4, local copies, waits for them, and re-layouts  3.93 us

commit v1 on v0

v1 whole, which is shorter than its diff:
```python
import functools

import jax
import jax.numpy as jnp
from jax import lax
from jax.experimental import pallas as pl
from jax.experimental.pallas import tpu as pltpu
from jax.sharding import PartitionSpec as P

epsilon = 1e-05
MESH = pl.DeviceIdType.MESH
F32 = jnp.float32
BF16 = jnp.bfloat16
PAD = 32
CHUNK = 256
PARTS = 2


def kernel(n, layers, taps_n, stream_in, gain, vw, gw, taps, cgain, ow, out,
           wvg, wo, nrm, gat, fil, act, ssend, srecv, dsend, drecv,
           asend, arecv, bsend, brecv, mine, through, strm,
           loc_sem, wx_send, wx_recv, z_send, z_recv, msg_send, msg_recv):
    planes = n // 4
    s = lax.axis_index("sp")
    c = lax.axis_index("tp")
    z, q = s // 4, s % 4
    y, x = q // 2, q % 2
    quad = [q, q + 1 - 2 * x, q + 2 - 4 * y, 3 - q]
    toks, width = stream_in.shape
    group = 4 * toks
    rows, cols = vw.shape[1], vw.shape[2]
    ch = cols // 4
    half = width // 2
    near = (1 - c) * quad[1] + c * quad[2]
    far = c * quad[1] + (1 - c) * quad[2]
    diag = quad[3]
    near_dev, far_dev, core_dev = (z * 4 + near, c), (z * 4 + far, c), (s, 1 - c)
    up_dev, down_dev = (s + 4, c), (s - 4, c)

    def al(v, m):
        return pl.multiple_of(v, m)

    barrier = pltpu.get_barrier_semaphore()
    plane_devs = [(z * 4 + quad[k], cc) for k in range(4) for cc in (c, 1 - c)][1:]
    for dev in plane_devs:
        pl.semaphore_signal(barrier, inc=1, device_id=dev, device_id_type=MESH)

    @pl.when(z < planes - 1)
    def _():
        pl.semaphore_signal(barrier, inc=1, device_id=up_dev, device_id_type=MESH)

    @pl.when(z > 0)
    def _():
        pl.semaphore_signal(barrier, inc=1, device_id=down_dev, device_id_type=MESH)

    pl.semaphore_wait(barrier, len(plane_devs) + (z < planes - 1).astype(jnp.int32)
                      + (z > 0).astype(jnp.int32))

    shared = {}

    def share(l, kind):
        mine_rows = pl.ds(al(s * rows, rows), rows)
        for k in range(4):
            span = pl.ds(al(quad[k] * ch, ch), ch)
            if kind == 2:
                src, dst = ow.at[l, span, :], wo.at[l, :, mine_rows]
            else:
                src = (vw, gw)[kind].at[l, :, span]
                dst = wvg.at[l, mine_rows, pl.ds(kind * ch, ch)]
            idx = l * 3 + kind
            if k == 0:
                copy = pltpu.make_async_copy(src, dst, loc_sem.at[idx])
            else:
                copy = pltpu.make_async_remote_copy(
                    src, dst, wx_send.at[idx, k], wx_recv.at[idx, k],
                    device_id=(z * 4 + quad[k], c), device_id_type=MESH)
            copy.start()
            shared[l, kind, k] = copy

    def z_copy(l, grp, d, t, hop, k):
        plane = z - t if d == 0 else z + t
        block = pl.ds(al((plane * 4 + quad[k]) * rows, rows), rows)
        ref = wvg.at[l, block, :] if grp == 0 else wo.at[l, :, block]
        idx = (l * 2 + grp) * 2 + d
        return pltpu.make_async_remote_copy(
            ref, ref, z_send.at[idx, hop, k], z_recv.at[idx, hop, k],
            device_id=up_dev if d == 0 else down_dev, device_id_type=MESH)

    def holds(d, t):
        return z >= t if d == 0 else z + t < planes

    def sends(d):
        return z < planes - 1 if d == 0 else z > 0

    sent = []

    def pump(l, grp, t):
        for k in range(4):
            if t == 0:
                for kind in ((0, 1) if grp == 0 else (2,)):
                    shared[l, kind, k].wait()
            for d in range(2):
                @pl.when(holds(d, t) & sends(d))
                def _(k=k, d=d):
                    if t > 0:
                        z_copy(l, grp, d, t, t - 1, k).wait_recv()
                    z_copy(l, grp, d, t, t, k).start()

                sent.append((l, grp, d, t, k))

    def consume(l, grp):
        for t in range(1, planes):
            for d in range(2):
                @pl.when(holds(d, t) & jnp.logical_not(sends(d)))
                def _(t=t, d=d):
                    for k in range(4):
                        z_copy(l, grp, d, t, t - 1, k).wait_recv()

    slots = [0]

    def make(src, dst, dev):
        slot = slots[0]
        slots[0] += 1
        return pltpu.make_async_remote_copy(src, dst, msg_send.at[slot], msg_recv.at[slot],
                                            device_id=dev, device_id_type=MESH)

    def message(src, dst, dev):
        m = make(src, dst, dev)
        m.start()
        return m

    share(0, 0)
    share(0, 1)

    def block_rows(b):
        return pl.ds(al(b * toks, toks), toks)

    def half_cols(h):
        return pl.ds(al(h * half, half), half)

    total_rows = PAD + group
    tile = max(v for v in range(16, 257, 16) if total_rows % v == 0)
    part_rows = group // PARTS
    lanes = 128
    chunks = half // CHUNK
    halos = []

    for l in range(layers):
        last_layer = l + 1 == layers
        source = stream_in if l == 0 else strm.at[l - 1]

        def norm_step(r, _):
            at = al(r * 64, 64)
            wide = source[pl.ds(at, 64), :].astype(F32)
            scale = lax.rsqrt(jnp.mean(wide * wide, axis=1, keepdims=True) + epsilon)
            nrm[l, pl.ds(al(PAD + q * toks + at, 32), 64), :] = (
                wide * scale * gain[l:l + 1, :]).astype(BF16)
            return 0

        lax.fori_loop(0, toks // 64, norm_step, 0)

        @pl.when(z == 0)
        def _():
            nrm[l, 0:PAD, :] = jnp.zeros((PAD, width), BF16)

        def spot(b):
            return nrm.at[l, pl.ds(al(PAD + b * toks, 32), toks), half_cols(c)]

        own_near = message(spot(q), spot(q), near_dev)
        own_far = message(spot(q), spot(q), far_dev)
        if l == 0:
            pump(0, 0, 0)
            share(0, 2)
        own_near.wait()
        passed = message(spot(near), spot(near), far_dev)
        relays = [message(spot(near), spot(near), core_dev)]
        if l == 0:
            pump(0, 0, 1)
            for ll in range(1, layers):
                for kind in range(3):
                    share(ll, kind)
        else:
            pump(l, 1, 1)
        own_far.wait()
        relays.append(message(spot(far), spot(far), core_dev))
        if l == 0:
            for t in range(2, planes - 1):
                pump(0, 0, t)
            pump(0, 1, 0)
        passed.wait()
        relays.append(message(spot(diag), spot(diag), core_dev))
        border = nrm.at[l, pl.ds(group, PAD), half_cols(c)]
        first = nrm.at[l, pl.ds(0, PAD), half_cols(c)]
        halo = make(border, first, up_dev)
        swap_halo = make(first, first, core_dev)
        halos.append(halo)

        @pl.when(z < planes - 1)
        def _():
            halo.start()

        if l > 0:
            for t in range(2, planes - 1):
                pump(l, 1, t)

        @pl.when(z > 0)
        def _():
            halo.wait_recv()
            swap_halo.start()

        for m in relays:
            m.wait()

        @pl.when(z > 0)
        def _():
            swap_halo.wait()

        consume(l, 0)

        def gate_step(r, _):
            at = al(r * tile, tile)
            both = jnp.dot(nrm[l, pl.ds(at, tile), :], wvg[l], preferred_element_type=F32)
            gated = (both[:, :ch] * jax.nn.sigmoid(both[:, ch:])).astype(BF16)
            gat[pl.ds(at, tile), :] = gated.astype(F32)
            return 0

        lax.fori_loop(0, total_rows // tile, gate_step, 0)
        if l == 0:
            pump(0, 1, 1)

        lead = PAD - (taps_n - 1)
        step_rows = 64

        def conv_step(r, _):
            at = al(r * step_rows, step_rows)
            for lane in range(ch // lanes):
                cut = slice(lane * lanes, (lane + 1) * lanes)
                total = jnp.zeros((step_rows, lanes), F32)
                block = gat[pl.ds(at, step_rows + PAD), cut]
                for b in range(8):
                    moved = block if b == 0 else pltpu.roll(block, step_rows + PAD - b, 0)
                    for a in range(PAD // 8 + 1):
                        tap = 8 * a + b - lead
                        if 0 <= tap < taps_n:
                            total = total + taps[l, tap:tap + 1, cut] * moved[8 * a:8 * a + step_rows]
                fil[pl.ds(at, step_rows), cut] = total
            return 0

        per = part_rows // step_rows
        sums = []
        for part in range(PARTS):
            lax.fori_loop(part * per, (part + 1) * per, conv_step, 0)
            wide = fil[part * part_rows:(part + 1) * part_rows, :]
            first_sum = jnp.sum(wide, axis=1, keepdims=True)
            second_sum = jnp.sum(wide * wide, axis=1, keepdims=True)
            lane_id = lax.broadcasted_iota(jnp.int32, (part_rows, lanes), 1)
            stat = jnp.where(lane_id == 0, first_sum, jnp.where(lane_id == 1, second_sum, 0.0))
            ssend[l, part] = jnp.transpose(stat)[0:8, :]
            sums.append([message(ssend.at[l, part], srecv.at[l, part, k], dev)
                         for k, dev in enumerate(plane_devs)])
            if l == 0 and part == 0:
                for t in range(2, planes - 1):
                    pump(0, 1, t)
        if not last_layer:
            pump(l + 1, 0, 0)
        for part in range(PARTS):
            span = slice(part * part_rows, (part + 1) * part_rows)
            for m in sums[part]:
                m.wait()
            whole = ssend[l, part]
            for k in range(len(plane_devs)):
                whole = whole + srecv[l, part, k]
            stat = jnp.transpose(jnp.concatenate(
                [whole, jnp.zeros((lanes - 8, part_rows), F32)], axis=0))
            mean_value = stat[:, 0:1] / width
            variance = stat[:, 1:2] / width - mean_value * mean_value
            act[span, :] = jax.nn.silu((fil[span, :] - mean_value) * lax.rsqrt(variance + epsilon)
                                       * cgain[l:l + 1, pl.ds(al(q * ch, ch), ch)]).astype(BF16)

        consume(l, 1)
        swaps, firsts, seconds, lasts = [], [], [], []

        def out_cols(h, u):
            return pl.ds(al(h * half + u * CHUNK, CHUNK), CHUNK)

        def stage_swap(u):
            weights = wo[l, :, out_cols(1 - c, u)]
            for b in range(4):
                span = slice(b * toks, (b + 1) * toks)
                dsend[l, u, span, :] = jnp.dot(act[span, :], weights,
                                               preferred_element_type=F32).astype(BF16)
            swaps.append(message(dsend.at[l, u], drecv.at[l, u], core_dev))

        def stage_first(u):
            weights = wo[l, :, out_cols(c, u)]
            swaps[u].wait()

            def partial(b):
                return (jnp.dot(act[block_rows(b), :], weights, preferred_element_type=F32)
                        + drecv[l, u, block_rows(b), :].astype(F32))

            asend[l, u, 0] = partial(far).astype(BF16)
            asend[l, u, 1] = partial(diag).astype(BF16)
            firsts.append(message(asend.at[l, u], arecv.at[l, u], far_dev))
            through[u] = partial(near)
            mine[u] = partial(q) + source[:, out_cols(c, u)].astype(F32)

        def stage_second(u):
            firsts[u].wait()
            bsend[l, u] = (through[u] + arecv[l, u, 1].astype(F32)).astype(BF16)
            seconds.append(message(bsend.at[l, u], brecv.at[l, u], near_dev))
            mine[u] = mine[u] + arecv[l, u, 0].astype(F32)

        def stage_last(u):
            seconds[u].wait()
            strm[l, :, out_cols(c, u)] = (mine[u] + brecv[l, u].astype(F32)).astype(BF16)
            piece = strm.at[l, :, out_cols(c, u)]
            lasts.append(message(piece, piece, core_dev))

        lag = 4
        for i in range(chunks + lag + 1):
            if i < chunks:
                stage_swap(i)
            if 1 <= i <= chunks:
                stage_first(i - 1)
            if 0 <= i - lag < chunks:
                stage_second(i - lag)
            if 0 <= i - lag - 1 < chunks:
                stage_last(i - lag - 1)
            if not last_layer and i == 1:
                pump(l + 1, 0, 1)
            if not last_layer and i == 6:
                for t in range(2, planes - 1):
                    pump(l + 1, 0, t)
                pump(l + 1, 1, 0)
        for m in lasts:
            m.wait()

    out[...] = strm[layers - 1]
    for l, grp, d, t, k in sent:
        @pl.when(holds(d, t) & sends(d))
        def _(l=l, grp=grp, d=d, t=t, k=k):
            z_copy(l, grp, d, t, t, k).wait_send()
    for halo in halos:
        @pl.when(z < planes - 1)
        def _(halo=halo):
            halo.wait_send()


def fused(n, layers):
    def body(stream_in, norm_gain, value_weight, gate_weight, conv_taps, channel_gain, out_weight):
        toks, width = stream_in.shape
        taps_n = conv_taps.shape[1]
        rows, cols = value_weight.shape[1], value_weight.shape[2]
        ch, half, group, planes = cols // 4, width // 2, 4 * toks, n // 4
        chunks = half // CHUNK
        q = lax.axis_index("sp") % 4
        taps = lax.dynamic_slice_in_dim(conv_taps, q * ch, ch, axis=2)
        vmem = pl.BlockSpec(memory_space=pltpu.VMEM)
        hbm = pl.BlockSpec(memory_space=pltpu.HBM)
        msgs = layers * (8 + 7 * PARTS + 4 * chunks)
        return pl.pallas_call(
            functools.partial(kernel, n, layers, taps_n),
            out_shape=jax.ShapeDtypeStruct((toks, width), BF16),
            in_specs=[vmem, vmem, hbm, hbm, vmem, vmem, hbm],
            out_specs=vmem,
            scratch_shapes=[
                pltpu.VMEM((layers, width, 2 * ch), BF16),
                pltpu.VMEM((layers, ch, width), BF16),
                pltpu.VMEM((layers, PAD + group, width), BF16),
                pltpu.VMEM((PAD + group, ch), F32),
                pltpu.VMEM((group, ch), F32),
                pltpu.VMEM((group, ch), BF16),
                pltpu.VMEM((layers, PARTS, 8, group // PARTS), F32),
                pltpu.VMEM((layers, PARTS, 7, 8, group // PARTS), F32),
                pltpu.VMEM((layers, chunks, group, CHUNK), BF16),
                pltpu.VMEM((layers, chunks, group, CHUNK), BF16),
                pltpu.VMEM((layers, chunks, 2, toks, CHUNK), BF16),
                pltpu.VMEM((layers, chunks, 2, toks, CHUNK), BF16),
                pltpu.VMEM((layers, chunks, toks, CHUNK), BF16),
                pltpu.VMEM((layers, chunks, toks, CHUNK), BF16),
                pltpu.VMEM((chunks, toks, CHUNK), F32),
                pltpu.VMEM((chunks, toks, CHUNK), F32),
                pltpu.VMEM((layers, toks, width), BF16),
                pltpu.SemaphoreType.DMA((layers * 3,)),
                pltpu.SemaphoreType.DMA((layers * 3, 4)),
                pltpu.SemaphoreType.DMA((layers * 3, 4)),
                pltpu.SemaphoreType.DMA((layers * 4, planes - 1, 4)),
                pltpu.SemaphoreType.DMA((layers * 4, planes - 1, 4)),
                pltpu.SemaphoreType.DMA((msgs,)),
                pltpu.SemaphoreType.DMA((msgs,)),
            ],
            compiler_params=pltpu.CompilerParams(
                collective_id=0, has_side_effects=True, vmem_limit_bytes=62 * 2**20),
        )(stream_in, norm_gain, value_weight, gate_weight, taps, channel_gain, out_weight)

    return body


def passed_along(value, axis, steps):
    count = lax.axis_size(axis)
    leading, last = (max(0, -steps), min(count, count - steps))
    return lax.ppermute(value, axis, [(source, source + steps) for source in range(leading, last)])


def general(stream_in, norm_gain, value_weight, gate_weight, conv_taps, channel_gain, out_weight):
    stream = stream_in
    tok_rows = stream_in.shape[0]
    width = stream_in.shape[1]
    taps_n = conv_taps.shape[1]
    local_cols = value_weight.shape[2]
    for layer in range(norm_gain.shape[0]):
        wide = stream.astype(F32)
        normed = (
            wide
            * lax.rsqrt(jnp.mean(wide * wide, axis=1, keepdims=True) + epsilon)
            * norm_gain[layer]
        ).astype(BF16)
        value = jnp.dot(normed, lax.all_gather(value_weight[layer], "sp", axis=0, tiled=True),
                        preferred_element_type=F32)
        gate = jnp.dot(normed, lax.all_gather(gate_weight[layer], "sp", axis=0, tiled=True),
                       preferred_element_type=F32)
        gated = (value * jax.nn.sigmoid(gate)).astype(BF16)
        earlier = passed_along(gated[tok_rows - (taps_n - 1):], "sp", 1)
        padded = jnp.concatenate([earlier, gated], axis=0).astype(F32)
        taps = conv_taps[layer]
        filtered = jnp.zeros((tok_rows, local_cols), F32)
        for tap in range(taps_n):
            filtered = filtered + taps[tap] * padded[tap:tap + tok_rows]
        sum_first, sum_second = lax.psum(
            (jnp.sum(filtered, axis=1), jnp.sum(filtered * filtered, axis=1)), "tp")
        mean_value = (sum_first / width)[:, None]
        variance = (sum_second / width)[:, None] - mean_value * mean_value
        activated = jax.nn.silu(
            (filtered - mean_value) * lax.rsqrt(variance + epsilon) * channel_gain[layer]
        ).astype(BF16)
        whole_out = lax.all_gather(out_weight[layer], "sp", axis=1, tiled=True)
        terms = jnp.dot(activated, whole_out, preferred_element_type=F32)
        summed = lax.psum(terms.astype(BF16), "tp").astype(F32)
        stream = (wide + summed).astype(BF16)
    return stream


def solution(mesh):
    n, tp = mesh.shape["sp"], mesh.shape["tp"]

    def body(stream_in, norm_gain, value_weight, *rest):
        rows, cols = value_weight.shape[1], value_weight.shape[2]
        quads = tp == 2 and n % 4 == 0 and n >= 8 and rows % 128 == 0 and cols % 512 == 0
        fits = (stream_in.shape[0] % 64 == 0 and rest[1].shape[1] <= PAD
                and stream_in.shape[1] % (2 * CHUNK) == 0)
        chosen = fused(n, norm_gain.shape[0]) if quads and fits else general
        return chosen(stream_in, norm_gain, value_weight, *rest)

    return jax.shard_map(
        body,
        mesh=mesh,
        in_specs=(
            P("sp", None),
            P(),
            P(None, "sp", "tp"),
            P(None, "sp", "tp"),
            P(None, None, "tp"),
            P(None, "tp"),
            P(None, "tp", "sp"),
        ),
        out_specs=P("sp", None),
        check_vma=False,
    )
```

time: 167 us -> 171 us (1.024)
  the two profiles are of different devices: /device:TPU:0 before, /device:TPU:29 now
where the time goes in v1:
time: 171 us
  Pallas kernels  167 us (98%)
  local copies, waits for them, and re-layouts  3.9 us (2%)
    pallas_call x1, Pallas kernels, body(): pl.pallas_call(functools.partial(kernel, n, layers, taps_n), out_shape=ja...  167 us
    unnamed x4, local copies, waits for them, and re-layouts  3.89 us

profile of v1, /device:TPU:29, one launch (start us, length us, event | category | flops | bytes accessed | tf_op | source)
XLA Modules:
  0.0 170.8 jit_solution(11084452789529183692)
XLA Ops:
  0.0 0.0 copy-start
  0.0 0.9 copy-done
  1.0 0.6 copy.9.taps
  1.6 166.9 %shard_map.73 = bf16[256,2048]{1,0:T(8,128)(2,1)} custom-call(bf16[256,2048]{1,0:T(8,128)(2,1)} %stream_in.1, f32[2,2048]{1,0:T(2,128)} %gain.1, bf16[2,128,1024]{2,1,0:T(8,128)(2,1)} %vw.1, bf16[2,128,1024]{2,1,0:T(8,128)(2,1)} %gw.1, f32[2,31,256]{2,1,0:T(8,128)} %copy.9.taps, f32[2,1024]{1,0:T(2,128)} %cgain.1, bf16[2,1024,128]{2,1,0:T(8,128)(2,1)} %ow.1), custom_call_target="tpu_custom_call" | custom-call | tf_op jit(solution)/shard_map/pallas_call | solution.py:362
  168.5 2.3 %copy.11 = bf16[256,2048]{1,0:T(8,128)(2,1)} copy(bf16[256,2048]{1,0:T(8,128)(2,1)} %shard_map.73) | data formatting | bytes 2097152
  (1 shorter events, 0.0 us)
Async XLA Ops:
  0.0 0.9 copy-start

commit v2 on v1

--- a/solution.py
+++ b/solution.py
@@ -12,14 +12,14 @@
 F32 = jnp.float32
 BF16 = jnp.bfloat16
 PAD = 32
-CHUNK = 256
 PARTS = 2
 
 
-def kernel(n, layers, taps_n, stream_in, gain, vw, gw, taps, cgain, ow, out,
-           wvg, wo, nrm, gat, fil, act, ssend, srecv, dsend, drecv,
+def kernel(n, layers, taps_n, stream_hbm, gain_hbm, vw, gw, taps_hbm, cgain_hbm, ow, out,
+           stream_in, gain, taps, cgain, wvg, wo, nrm, gat, fil, act, ssend, srecv, dsend, drecv,
            asend, arecv, bsend, brecv, mine, through, strm,
-           loc_sem, wx_send, wx_recv, z_send, z_recv, msg_send, msg_recv):
+           in_sem, out_sem, loc_sem, wx_send, wx_recv, z_send, z_recv, halo_send, halo_recv,
+           msg_send, msg_recv):
     planes = n // 4
     s = lax.axis_index("sp")
     c = lax.axis_index("tp")
@@ -31,6 +31,7 @@
     rows, cols = vw.shape[1], vw.shape[2]
     ch = cols // 4
     half = width // 2
+    chunk = 2 * rows
     near = (1 - c) * quad[1] + c * quad[2]
     far = c * quad[1] + (1 - c) * quad[2]
     diag = quad[3]
@@ -53,38 +54,60 @@
     def _():
         pl.semaphore_signal(barrier, inc=1, device_id=down_dev, device_id_type=MESH)
 
+    own_ch = pl.ds(al(q * ch, ch), ch)
+    loads = [pltpu.make_async_copy(a, b, in_sem.at[k]) for k, (a, b) in enumerate((
+        (stream_hbm, stream_in), (gain_hbm, gain), (taps_hbm.at[:, :, own_ch], taps),
+        (cgain_hbm.at[:, own_ch], cgain)))]
+    for load in loads:
+        load.start()
+
+    shared = {}
+
+    def shared_copy(l, kind, k):
+        mine_rows = pl.ds(al(s * rows, rows), rows)
+        span = pl.ds(al(quad[k] * ch, ch), ch)
+        if kind == 2:
+            src, dst = ow.at[l, span, :], wo.at[l, :, mine_rows]
+        else:
+            src = (vw, gw)[kind].at[l, :, span]
+            dst = wvg.at[l, mine_rows, pl.ds(kind * ch, ch)]
+        idx = l * 3 + kind
+        if k == 0:
+            copy = pltpu.make_async_copy(src, dst, loc_sem.at[idx])
+        else:
+            copy = pltpu.make_async_remote_copy(
+                src, dst, wx_send.at[idx, k], wx_recv.at[idx, k],
+                device_id=(z * 4 + quad[k], c), device_id_type=MESH)
+        copy.start()
+        shared[l, kind, k] = copy
+
+    def share(l, kinds, ks=(1, 2, 3)):
+        for k in ks:
+            for kind in kinds:
+                shared_copy(l, kind, k)
+
+    for l in range(layers):
+        share(l, (0, 1, 2), (0,))
+
     pl.semaphore_wait(barrier, len(plane_devs) + (z < planes - 1).astype(jnp.int32)
                       + (z > 0).astype(jnp.int32))
 
-    shared = {}
-
-    def share(l, kind):
-        mine_rows = pl.ds(al(s * rows, rows), rows)
-        for k in range(4):
-            span = pl.ds(al(quad[k] * ch, ch), ch)
-            if kind == 2:
-                src, dst = ow.at[l, span, :], wo.at[l, :, mine_rows]
-            else:
-                src = (vw, gw)[kind].at[l, :, span]
-                dst = wvg.at[l, mine_rows, pl.ds(kind * ch, ch)]
-            idx = l * 3 + kind
-            if k == 0:
-                copy = pltpu.make_async_copy(src, dst, loc_sem.at[idx])
-            else:
-                copy = pltpu.make_async_remote_copy(
-                    src, dst, wx_send.at[idx, k], wx_recv.at[idx, k],
-                    device_id=(z * 4 + quad[k], c), device_id_type=MESH)
-            copy.start()
-            shared[l, kind, k] = copy
-
     def z_copy(l, grp, d, t, hop, k):
         plane = z - t if d == 0 else z + t
-        block = pl.ds(al((plane * 4 + quad[k]) * rows, rows), rows)
+        if k < 0:
+            block = pl.ds(al(plane * 4 * rows, rows), 4 * rows)
+        elif l == 0:
+            block = pl.ds(al((plane * 4 + quad[k]) * rows, rows), rows)
+        else:
+            block = pl.ds(al((plane * 4 + 2 * k) * rows, rows), 2 * rows)
         ref = wvg.at[l, block, :] if grp == 0 else wo.at[l, :, block]
         idx = (l * 2 + grp) * 2 + d
         return pltpu.make_async_remote_copy(
-            ref, ref, z_send.at[idx, hop, k], z_recv.at[idx, hop, k],
+            ref, ref, z_send.at[idx, hop], z_recv.at[idx, hop, max(k, 0)],
             device_id=up_dev if d == 0 else down_dev, device_id_type=MESH)
+
+    def pieces(l):
+        return 4 if l == 0 else 2
 
     def holds(d, t):
         return z >= t if d == 0 else z + t < planes
@@ -92,12 +115,15 @@
     def sends(d):
         return z < planes - 1 if d == 0 else z > 0
 
-    sent = []
-
     def pump(l, grp, t):
-        for k in range(4):
-            if t == 0:
-                for kind in ((0, 1) if grp == 0 else (2,)):
+        kinds = (0, 1) if grp == 0 else (2,)
+        if t == 0 and l > 0:
+            for k in range(4):
+                for kind in kinds:
+                    shared[l, kind, k].wait()
+        for k in range(pieces(l)):
+            if t == 0 and l == 0:
+                for kind in kinds:
                     shared[l, kind, k].wait()
             for d in range(2):
                 @pl.when(holds(d, t) & sends(d))
@@ -106,15 +132,19 @@
                         z_copy(l, grp, d, t, t - 1, k).wait_recv()
                     z_copy(l, grp, d, t, t, k).start()
 
-                sent.append((l, grp, d, t, k))
-
-    def consume(l, grp):
-        for t in range(1, planes):
+    def consume(l, grp, t):
+        for d in range(2):
+            @pl.when(holds(d, t) & jnp.logical_not(sends(d)))
+            def _(d=d):
+                for k in range(pieces(l)):
+                    z_copy(l, grp, d, t, t - 1, k).wait_recv()
+
+    def drain(l, grp):
+        for t in range(planes - 1):
             for d in range(2):
-                @pl.when(holds(d, t) & jnp.logical_not(sends(d)))
+                @pl.when(holds(d, t) & sends(d))
                 def _(t=t, d=d):
-                    for k in range(4):
-                        z_copy(l, grp, d, t, t - 1, k).wait_recv()
+                    z_copy(l, grp, d, t, t, -1).wait_send()
 
     slots = [0]
 
@@ -129,8 +159,9 @@
         m.start()
         return m
 
-    share(0, 0)
-    share(0, 1)
+    share(0, (0, 1))
+    for load in loads:
+        load.wait()
 
     def block_rows(b):
         return pl.ds(al(b * toks, toks), toks)
@@ -138,12 +169,16 @@
     def half_cols(h):
         return pl.ds(al(h * half, half), half)
 
-    total_rows = PAD + group
-    tile = max(v for v in range(16, 257, 16) if total_rows % v == 0)
+    unit = toks // 2
     part_rows = group // PARTS
     lanes = 128
-    chunks = half // CHUNK
-    halos = []
+    outs = []
+
+    def plane_at(u):
+        low = jnp.where(u <= z, z - u, u)
+        zm = planes - 1 - z
+        high = planes - 1 - jnp.where(u <= zm, zm - u, u)
+        return jnp.where(2 * z < planes, low, high)
 
     for l in range(layers):
         last_layer = l + 1 == layers
@@ -163,70 +198,131 @@
         def _():
             nrm[l, 0:PAD, :] = jnp.zeros((PAD, width), BF16)
 
-        def spot(b):
-            return nrm.at[l, pl.ds(al(PAD + b * toks, 32), toks), half_cols(c)]
-
-        own_near = message(spot(q), spot(q), near_dev)
-        own_far = message(spot(q), spot(q), far_dev)
+        def spot(b, j):
+            return nrm.at[l, pl.ds(al(PAD + b * toks + j * unit, 32), unit), half_cols(c)]
+
+        border = nrm.at[l, pl.ds(group, PAD), half_cols(c)]
+        first = nrm.at[l, pl.ds(0, PAD), half_cols(c)]
+
+        def halo_copy(k, dev, src, recv):
+            return pltpu.make_async_remote_copy(
+                src, first, halo_send.at[l, k], halo_recv.at[l, recv],
+                device_id=dev, device_id_type=MESH)
+
+        rise = halo_copy(0, up_dev, border, 0)
+        spread = [halo_copy(k, (z * 4 + quad[k], c), first, 1) for k in (1, 2, 3)]
+        swap_halo = halo_copy(4, core_dev, first, 2)
+
+        @pl.when((q == 3) & (z < planes - 1))
+        def _():
+            rise.start()
+
+        def halo_spread():
+            @pl.when((q == 3) & (z > 0))
+            def _():
+                rise.wait_recv()
+                for m in spread:
+                    m.start()
+                swap_halo.start()
+
+        def halo_swap():
+            @pl.when((q != 3) & (z > 0))
+            def _():
+                spread[0].wait_recv()
+                swap_halo.start()
+
+        def halo_finish():
+            @pl.when(z > 0)
+            def _():
+                swap_halo.wait()
+
+            @pl.when((q == 3) & (z > 0))
+            def _():
+                for m in spread:
+                    m.wait_send()
+
+            @pl.when((q == 3) & (z < planes - 1))
+            def _():
+                rise.wait_send()
+
+        own_near = [message(spot(q, j), spot(q, j), near_dev) for j in range(2)]
+        passed, relays, own_far = [], {}, []
+
+        def to_far(j):
+            own_near[j].wait_send()
+            own_far.append(message(spot(q, j), spot(q, j), far_dev))
+
+        def pass_on(j):
+            own_near[j].wait_recv()
+            passed.append(message(spot(near, j), spot(near, j), far_dev))
+            relays[1, j] = message(spot(near, j), spot(near, j), core_dev)
+
+        def relay(which, j):
+            (own_far if which == 2 else passed)[j].wait()
+            b = far if which == 2 else diag
+            relays[which, j] = message(spot(b, j), spot(b, j), core_dev)
+
+        def gate_rows(at, size):
+            both = jnp.dot(nrm[l, pl.ds(at, size), :], wvg[l], preferred_element_type=F32)
+            gated = (both[:, :ch] * jax.nn.sigmoid(both[:, ch:])).astype(BF16)
+            gat[pl.ds(at, size), :] = gated.astype(F32)
+
+        def gate_pair(which, j):
+            b = (q, near, far, diag)[which]
+            gate_rows(al(PAD + b * toks + j * unit, 32), unit)
+
         if l == 0:
             pump(0, 0, 0)
-            share(0, 2)
-        own_near.wait()
-        passed = message(spot(near), spot(near), far_dev)
-        relays = [message(spot(near), spot(near), core_dev)]
-        if l == 0:
+            halo_spread()
+            to_far(0)
+            to_far(1)
             pump(0, 0, 1)
-            for ll in range(1, layers):
-                for kind in range(3):
-                    share(ll, kind)
-        else:
-            pump(l, 1, 1)
-        own_far.wait()
-        relays.append(message(spot(far), spot(far), core_dev))
-        if l == 0:
+            pass_on(0)
+            pass_on(1)
+            share(0, (2,))
+            relay(2, 0)
+            relay(2, 1)
             for t in range(2, planes - 1):
                 pump(0, 0, t)
+            relay(3, 0)
+            relay(3, 1)
+            for ll in range(1, layers):
+                share(ll, (0, 1, 2))
             pump(0, 1, 0)
-        passed.wait()
-        relays.append(message(spot(diag), spot(diag), core_dev))
-        border = nrm.at[l, pl.ds(group, PAD), half_cols(c)]
-        first = nrm.at[l, pl.ds(0, PAD), half_cols(c)]
-        halo = make(border, first, up_dev)
-        swap_halo = make(first, first, core_dev)
-        halos.append(halo)
-
-        @pl.when(z < planes - 1)
-        def _():
-            halo.start()
-
-        if l > 0:
-            for t in range(2, planes - 1):
-                pump(l, 1, t)
-
-        @pl.when(z > 0)
-        def _():
-            halo.wait_recv()
-            swap_halo.start()
-
-        for m in relays:
-            m.wait()
-
-        @pl.when(z > 0)
-        def _():
-            swap_halo.wait()
-
-        consume(l, 0)
-
-        def gate_step(r, _):
-            at = al(r * tile, tile)
-            both = jnp.dot(nrm[l, pl.ds(at, tile), :], wvg[l], preferred_element_type=F32)
-            gated = (both[:, :ch] * jax.nn.sigmoid(both[:, ch:])).astype(BF16)
-            gat[pl.ds(at, tile), :] = gated.astype(F32)
-            return 0
-
-        lax.fori_loop(0, total_rows // tile, gate_step, 0)
-        if l == 0:
             pump(0, 1, 1)
+            halo_swap()
+            for m in relays.values():
+                m.wait()
+            for t in range(1, planes):
+                consume(0, 0, t)
+            for which in range(4):
+                for j in range(2):
+                    gate_pair(which, j)
+        else:
+            to_far(0)
+            to_far(1)
+            pass_on(0)
+            pass_on(1)
+            halo_spread()
+            pump(l, 1, 1)
+            relay(2, 0)
+            relay(2, 1)
+            drain(l - 1, 0)
+            drain(l - 1, 1)
+            relay(3, 0)
+            relay(3, 1)
+            for t in range(1, planes):
+                consume(l, 0, t)
+            gate_pair(0, 0)
+            gate_pair(0, 1)
+            halo_swap()
+            for m in relays.values():
+                m.wait()
+            for which in range(1, 4):
+                for j in range(2):
+                    gate_pair(which, j)
+        halo_finish()
+        gate_rows(0, PAD)
 
         lead = PAD - (taps_n - 1)
         step_rows = 64
@@ -242,7 +338,7 @@
                     for a in range(PAD // 8 + 1):
                         tap = 8 * a + b - lead
                         if 0 <= tap < taps_n:
-                            total = total + taps[l, tap:tap + 1, cut] * moved[8 * a:8 * a + step_rows]
+                            total = total + taps[tap, l:l + 1, cut] * moved[8 * a:8 * a + step_rows]
                 fil[pl.ds(at, step_rows), cut] = total
             return 0
 
@@ -258,9 +354,8 @@
             ssend[l, part] = jnp.transpose(stat)[0:8, :]
             sums.append([message(ssend.at[l, part], srecv.at[l, part, k], dev)
                          for k, dev in enumerate(plane_devs)])
-            if l == 0 and part == 0:
-                for t in range(2, planes - 1):
-                    pump(0, 1, t)
+        for t in range(2, planes - 1):
+            pump(l, 1, t)
         if not last_layer:
             pump(l + 1, 0, 0)
         for part in range(PARTS):
@@ -275,15 +370,16 @@
             mean_value = stat[:, 0:1] / width
             variance = stat[:, 1:2] / width - mean_value * mean_value
             act[span, :] = jax.nn.silu((fil[span, :] - mean_value) * lax.rsqrt(variance + epsilon)
-                                       * cgain[l:l + 1, pl.ds(al(q * ch, ch), ch)]).astype(BF16)
-
-        consume(l, 1)
+                                       * cgain[l:l + 1, :]).astype(BF16)
+
         swaps, firsts, seconds, lasts = [], [], [], []
 
         def out_cols(h, u):
-            return pl.ds(al(h * half + u * CHUNK, CHUNK), CHUNK)
+            return pl.ds(al(plane_at(u) * 4 * rows + h * chunk, chunk), chunk)
 
         def stage_swap(u):
+            if u > 0:
+                consume(l, 1, u)
             weights = wo[l, :, out_cols(1 - c, u)]
             for b in range(4):
                 span = slice(b * toks, (b + 1) * toks)
@@ -316,16 +412,26 @@
             strm[l, :, out_cols(c, u)] = (mine[u] + brecv[l, u].astype(F32)).astype(BF16)
             piece = strm.at[l, :, out_cols(c, u)]
             lasts.append(message(piece, piece, core_dev))
+            if last_layer:
+                outs.append(pltpu.make_async_copy(piece, out.at[:, out_cols(c, u)], out_sem.at[0, u]))
+                outs[-1].start()
+
+        def finish(u):
+            lasts[u].wait()
+            if last_layer:
+                outs.append(pltpu.make_async_copy(
+                    strm.at[l, :, out_cols(1 - c, u)], out.at[:, out_cols(1 - c, u)], out_sem.at[1, u]))
+                outs[-1].start()
 
         lag = 4
-        for i in range(chunks + lag + 1):
-            if i < chunks:
+        for i in range(planes + lag + 1):
+            if i < planes:
                 stage_swap(i)
-            if 1 <= i <= chunks:
+            if 1 <= i <= planes:
                 stage_first(i - 1)
-            if 0 <= i - lag < chunks:
+            if 0 <= i - lag < planes:
                 stage_second(i - lag)
-            if 0 <= i - lag - 1 < chunks:
+            if 0 <= i - lag - 1 < planes:
                 stage_last(i - lag - 1)
             if not last_layer and i == 1:
                 pump(l + 1, 0, 1)
@@ -333,18 +439,14 @@
                 for t in range(2, planes - 1):
                     pump(l + 1, 0, t)
                 pump(l + 1, 1, 0)
-        for m in lasts:
-            m.wait()
-
-    out[...] = strm[layers - 1]
-    for l, grp, d, t, k in sent:
-        @pl.when(holds(d, t) & sends(d))
-        def _(l=l, grp=grp, d=d, t=t, k=k):
-            z_copy(l, grp, d, t, t, k).wait_send()
-    for halo in halos:
-        @pl.when(z < planes - 1)
-        def _(halo=halo):
-            halo.wait_send()
+            if last_layer and i == planes:
+                drain(l, 0)
+                drain(l, 1)
+        for u in range(planes):
+            finish(u)
+
+    for copy in outs:
+        copy.wait()
 
 
 def fused(n, layers):
@@ -353,18 +455,20 @@
         taps_n = conv_taps.shape[1]
         rows, cols = value_weight.shape[1], value_weight.shape[2]
         ch, half, group, planes = cols // 4, width // 2, 4 * toks, n // 4
-        chunks = half // CHUNK
-        q = lax.axis_index("sp") % 4
-        taps = lax.dynamic_slice_in_dim(conv_taps, q * ch, ch, axis=2)
-        vmem = pl.BlockSpec(memory_space=pltpu.VMEM)
+        chunk = 2 * rows
+        taps = jnp.transpose(conv_taps, (1, 0, 2))
         hbm = pl.BlockSpec(memory_space=pltpu.HBM)
-        msgs = layers * (8 + 7 * PARTS + 4 * chunks)
+        msgs = layers * (12 + 7 * PARTS + 4 * planes)
         return pl.pallas_call(
             functools.partial(kernel, n, layers, taps_n),
             out_shape=jax.ShapeDtypeStruct((toks, width), BF16),
-            in_specs=[vmem, vmem, hbm, hbm, vmem, vmem, hbm],
-            out_specs=vmem,
+            in_specs=[hbm] * 7,
+            out_specs=hbm,
             scratch_shapes=[
+                pltpu.VMEM((toks, width), BF16),
+                pltpu.VMEM((layers, width), F32),
+                pltpu.VMEM((taps_n, layers, ch), F32),
+                pltpu.VMEM((layers, ch), F32),
                 pltpu.VMEM((layers, width, 2 * ch), BF16),
                 pltpu.VMEM((layers, ch, width), BF16),
                 pltpu.VMEM((layers, PAD + group, width), BF16),
@@ -373,20 +477,24 @@
                 pltpu.VMEM((group, ch), BF16),
                 pltpu.VMEM((layers, PARTS, 8, group // PARTS), F32),
                 pltpu.VMEM((layers, PARTS, 7, 8, group // PARTS), F32),
-                pltpu.VMEM((layers, chunks, group, CHUNK), BF16),
-                pltpu.VMEM((layers, chunks, group, CHUNK), BF16),
-                pltpu.VMEM((layers, chunks, 2, toks, CHUNK), BF16),
-                pltpu.VMEM((layers, chunks, 2, toks, CHUNK), BF16),
-                pltpu.VMEM((layers, chunks, toks, CHUNK), BF16),
-                pltpu.VMEM((layers, chunks, toks, CHUNK), BF16),
-                pltpu.VMEM((chunks, toks, CHUNK), F32),
-                pltpu.VMEM((chunks, toks, CHUNK), F32),
+                pltpu.VMEM((layers, planes, group, chunk), BF16),
+                pltpu.VMEM((layers, planes, group, chunk), BF16),
+                pltpu.VMEM((layers, planes, 2, toks, chunk), BF16),
+                pltpu.VMEM((layers, planes, 2, toks, chunk), BF16),
+                pltpu.VMEM((layers, planes, toks, chunk), BF16),
+                pltpu.VMEM((layers, planes, toks, chunk), BF16),
+                pltpu.VMEM((planes, toks, chunk), F32),
+                pltpu.VMEM((planes, toks, chunk), F32),
                 pltpu.VMEM((layers, toks, width), BF16),
+                pltpu.SemaphoreType.DMA((4,)),
+                pltpu.SemaphoreType.DMA((2, planes)),
                 pltpu.SemaphoreType.DMA((layers * 3,)),
                 pltpu.SemaphoreType.DMA((layers * 3, 4)),
                 pltpu.SemaphoreType.DMA((layers * 3, 4)),
+                pltpu.SemaphoreType.DMA((layers * 4, planes - 1)),
                 pltpu.SemaphoreType.DMA((layers * 4, planes - 1, 4)),
-                pltpu.SemaphoreType.DMA((layers * 4, planes - 1, 4)),
+                pltpu.SemaphoreType.DMA((layers, 5)),
+                pltpu.SemaphoreType.DMA((layers, 3)),
                 pltpu.SemaphoreType.DMA((msgs,)),
                 pltpu.SemaphoreType.DMA((msgs,)),
             ],
@@ -447,8 +555,7 @@
     def body(stream_in, norm_gain, value_weight, *rest):
         rows, cols = value_weight.shape[1], value_weight.shape[2]
         quads = tp == 2 and n % 4 == 0 and n >= 8 and rows % 128 == 0 and cols % 512 == 0
-        fits = (stream_in.shape[0] % 64 == 0 and rest[1].shape[1] <= PAD
-                and stream_in.shape[1] % (2 * CHUNK) == 0)
+        fits = stream_in.shape[0] % 64 == 0 and rest[1].shape[1] <= PAD
         chosen = fused(n, norm_gain.shape[0]) if quads and fits else general
         return chosen(stream_in, norm_gain, value_weight, *rest)
 

time: 171 us -> 146 us (0.85)
  the two profiles are of different devices: /device:TPU:29 before, /device:TPU:0 now
where the time goes in v2:
time: 146 us; the launch traced here: 144 us
  Pallas kernels  142 us (97%)
  local copies, waits for them, and re-layouts  2.3 us (2%)
    pallas_call x1, Pallas kernels, body(): pl.pallas_call(functools.partial(kernel, n, layers, taps_n), out_shape=ja...  142 us

profile of v2, /device:TPU:0, one launch (start us, length us, event | category | flops | bytes accessed | tf_op | source)
XLA Modules:
  0.0 144.5 jit_solution(16959878074223969258)
XLA Ops:
  0.0 142.2 %shard_map.73 = bf16[256,2048]{1,0:T(8,128)(2,1)} custom-call(bf16[256,2048]{1,0:T(8,128)(2,1)} %stream_hbm.1, f32[2,2048]{1,0:T(2,128)} %gain_hbm.1, bf16[2,128,1024]{2,1,0:T(8,128)(2,1)} %vw.1, bf16[2,128,1024]{2,1,0:T(8,128)(2,1)} %gw.1, f32[31,2,1024]{2,1,0:T(2,128)} %bitcast.1, f32[2,1024]{1,0:T(2,128)} %cgain_hbm.1, bf16[2,1024,128]{2,1,0:T(8,128)(2,1)} %ow.1), custom_call_target="tpu_custom_call" | custom-call | tf_op jit(solution)/shard_map/pallas_call | solution.py:462
  142.2 2.3 %copy.9 = bf16[256,2048]{1,0:T(8,128)(2,1)} copy(bf16[256,2048]{1,0:T(8,128)(2,1)} %shard_map.73) | data formatting | bytes 2097152

commit v3 on v2

--- a/solution.py
+++ b/solution.py
@@ -17,7 +17,7 @@
 
 def kernel(n, layers, taps_n, stream_hbm, gain_hbm, vw, gw, taps_hbm, cgain_hbm, ow, out,
            stream_in, gain, taps, cgain, wvg, wo, nrm, gat, fil, act, ssend, srecv, dsend, drecv,
-           asend, arecv, bsend, brecv, mine, through, strm,
+           asend, arecv, bsend, brecv, mine, through, strm, acc, turn,
            in_sem, out_sem, loc_sem, wx_send, wx_recv, z_send, z_recv, halo_send, halo_recv,
            msg_send, msg_recv):
     planes = n // 4
@@ -76,7 +76,7 @@
             copy = pltpu.make_async_copy(src, dst, loc_sem.at[idx])
         else:
             copy = pltpu.make_async_remote_copy(
-                src, dst, wx_send.at[idx, k], wx_recv.at[idx, k],
+                src, dst, wx_send.at[idx, k - 1], wx_recv.at[idx, k - 1],
                 device_id=(z * 4 + quad[k], c), device_id_type=MESH)
         copy.start()
         shared[l, kind, k] = copy
@@ -96,18 +96,21 @@
         plane = z - t if d == 0 else z + t
         if k < 0:
             block = pl.ds(al(plane * 4 * rows, rows), 4 * rows)
-        elif l == 0:
+        elif pieces(l, grp) == 4:
             block = pl.ds(al((plane * 4 + quad[k]) * rows, rows), rows)
         else:
             block = pl.ds(al((plane * 4 + 2 * k) * rows, rows), 2 * rows)
         ref = wvg.at[l, block, :] if grp == 0 else wo.at[l, :, block]
         idx = (l * 2 + grp) * 2 + d
         return pltpu.make_async_remote_copy(
-            ref, ref, z_send.at[idx, hop], z_recv.at[idx, hop, max(k, 0)],
+            ref, ref, z_send.at[idx, hop], z_recv.at[first_recv(l, grp) + (d * (planes - 1) + hop) * pieces(l, grp) + max(k, 0)],
             device_id=up_dev if d == 0 else down_dev, device_id_type=MESH)
 
-    def pieces(l):
-        return 4 if l == 0 else 2
+    def pieces(l, grp):
+        return 4 if (l, grp) == (0, 0) else 2
+
+    def first_recv(l, grp):
+        return 2 * (planes - 1) * sum(pieces(*divmod(i, 2)) for i in range(l * 2 + grp))
 
     def holds(d, t):
         return z >= t if d == 0 else z + t < planes
@@ -117,12 +120,12 @@
 
     def pump(l, grp, t):
         kinds = (0, 1) if grp == 0 else (2,)
-        if t == 0 and l > 0:
+        if t == 0 and pieces(l, grp) == 2:
             for k in range(4):
                 for kind in kinds:
                     shared[l, kind, k].wait()
-        for k in range(pieces(l)):
-            if t == 0 and l == 0:
+        for k in range(pieces(l, grp)):
+            if t == 0 and pieces(l, grp) == 4:
                 for kind in kinds:
                     shared[l, kind, k].wait()
             for d in range(2):
@@ -132,12 +135,17 @@
                         z_copy(l, grp, d, t, t - 1, k).wait_recv()
                     z_copy(l, grp, d, t, t, k).start()
 
+    def consume_one(l, grp, t, d):
+        @pl.when(jnp.logical_not(sends(d)))
+        def _():
+            for k in range(pieces(l, grp)):
+                z_copy(l, grp, d, t, t - 1, k).wait_recv()
+
     def consume(l, grp, t):
         for d in range(2):
-            @pl.when(holds(d, t) & jnp.logical_not(sends(d)))
+            @pl.when(holds(d, t))
             def _(d=d):
-                for k in range(pieces(l)):
-                    z_copy(l, grp, d, t, t - 1, k).wait_recv()
+                consume_one(l, grp, t, d)
 
     def drain(l, grp):
         for t in range(planes - 1):
@@ -146,6 +154,7 @@
                 def _(t=t, d=d):
                     z_copy(l, grp, d, t, t, -1).wait_send()
 
+    turn[...] = jnp.zeros_like(turn)
     slots = [0]
 
     def make(src, dst, dev):
@@ -170,9 +179,10 @@
         return pl.ds(al(h * half, half), half)
 
     unit = toks // 2
+    total_rows = PAD + group
+    tile = max(v for v in range(16, 401, 16) if total_rows % v == 0)
     part_rows = group // PARTS
     lanes = 128
-    outs = []
 
     def plane_at(u):
         low = jnp.where(u <= z, z - u, u)
@@ -182,6 +192,7 @@
 
     for l in range(layers):
         last_layer = l + 1 == layers
+        slots[0] = 0
         source = stream_in if l == 0 else strm.at[l - 1]
 
         def norm_step(r, _):
@@ -266,6 +277,17 @@
             both = jnp.dot(nrm[l, pl.ds(at, size), :], wvg[l], preferred_element_type=F32)
             gated = (both[:, :ch] * jax.nn.sigmoid(both[:, ch:])).astype(BF16)
             gat[pl.ds(at, size), :] = gated.astype(F32)
+
+        def gate_part(t, plane):
+            depth = pl.ds(al(plane * 4 * rows, 4 * rows), 4 * rows)
+
+            def gate_step(r, _):
+                at = pl.ds(al(r * tile, 16), tile)
+                term = jnp.dot(nrm[l, at, depth], wvg[l, depth, :], preferred_element_type=F32)
+                acc[at, :] = term if t == 0 else acc[at, :] + term
+                return 0
+
+            lax.fori_loop(0, total_rows // tile, gate_step, 0)
 
         def gate_pair(which, j):
             b = (q, near, far, diag)[which]
@@ -289,40 +311,60 @@
             for ll in range(1, layers):
                 share(ll, (0, 1, 2))
             pump(0, 1, 0)
-            pump(0, 1, 1)
             halo_swap()
             for m in relays.values():
                 m.wait()
+            halo_finish()
+            gate_part(0, z)
             for t in range(1, planes):
-                consume(0, 0, t)
-            for which in range(4):
-                for j in range(2):
-                    gate_pair(which, j)
+                for d in range(2):
+                    @pl.when(holds(d, t))
+                    def _(t=t, d=d):
+                        consume_one(0, 0, t, d)
+                        gate_part(t, z - t if d == 0 else z + t)
+
+            def gate_end(r, _):
+                at = pl.ds(al(r * tile, 16), tile)
+                gated = (acc[at, :ch] * jax.nn.sigmoid(acc[at, ch:])).astype(BF16)
+                gat[at, :] = gated.astype(F32)
+                return 0
+
+            lax.fori_loop(0, total_rows // tile, gate_end, 0)
+            pump(0, 1, 1)
         else:
+            for t in range(2, planes - 1):
+                pump(l, 0, t)
+            halo_spread()
             to_far(0)
             to_far(1)
+            pump(l, 1, 0)
             pass_on(0)
             pass_on(1)
-            halo_spread()
-            pump(l, 1, 1)
-            relay(2, 0)
-            relay(2, 1)
-            drain(l - 1, 0)
-            drain(l - 1, 1)
-            relay(3, 0)
-            relay(3, 1)
             for t in range(1, planes):
                 consume(l, 0, t)
             gate_pair(0, 0)
             gate_pair(0, 1)
+            for j in range(2):
+                relay(2, j)
+                relays[1, j].wait()
+                gate_pair(2, j)
+            drain(l - 1, 0)
+            pump(l, 1, 1)
+            relay(3, 0)
+            relays[2, 0].wait()
+            gate_pair(1, 0)
+            relay(3, 1)
             halo_swap()
-            for m in relays.values():
-                m.wait()
-            for which in range(1, 4):
-                for j in range(2):
-                    gate_pair(which, j)
-        halo_finish()
-        gate_rows(0, PAD)
+            relays[2, 1].wait()
+            gate_pair(1, 1)
+            for j in range(2):
+                relays[3, j].wait()
+                gate_pair(3, j)
+            for t in range(2, planes - 1):
+                pump(l, 1, t)
+            halo_finish()
+            gate_rows(0, PAD)
+            drain(l - 1, 1)
 
         lead = PAD - (taps_n - 1)
         step_rows = 64
@@ -351,11 +393,12 @@
             second_sum = jnp.sum(wide * wide, axis=1, keepdims=True)
             lane_id = lax.broadcasted_iota(jnp.int32, (part_rows, lanes), 1)
             stat = jnp.where(lane_id == 0, first_sum, jnp.where(lane_id == 1, second_sum, 0.0))
-            ssend[l, part] = jnp.transpose(stat)[0:8, :]
+            ssend[l, part] = jnp.transpose(stat)[0:2, :]
             sums.append([message(ssend.at[l, part], srecv.at[l, part, k], dev)
                          for k, dev in enumerate(plane_devs)])
-        for t in range(2, planes - 1):
-            pump(l, 1, t)
+        if l == 0:
+            for t in range(2, planes - 1):
+                pump(l, 1, t)
         if not last_layer:
             pump(l + 1, 0, 0)
         for part in range(PARTS):
@@ -365,15 +408,13 @@
             whole = ssend[l, part]
             for k in range(len(plane_devs)):
                 whole = whole + srecv[l, part, k]
-            stat = jnp.transpose(jnp.concatenate(
-                [whole, jnp.zeros((lanes - 8, part_rows), F32)], axis=0))
+            turn[0:2, :] = whole
+            stat = jnp.transpose(turn[...])
             mean_value = stat[:, 0:1] / width
             variance = stat[:, 1:2] / width - mean_value * mean_value
             act[span, :] = jax.nn.silu((fil[span, :] - mean_value) * lax.rsqrt(variance + epsilon)
                                        * cgain[l:l + 1, :]).astype(BF16)
 
-        swaps, firsts, seconds, lasts = [], [], [], []
-
         def out_cols(h, u):
             return pl.ds(al(plane_at(u) * 4 * rows + h * chunk, chunk), chunk)
 
@@ -381,72 +422,78 @@
             if u > 0:
                 consume(l, 1, u)
             weights = wo[l, :, out_cols(1 - c, u)]
-            for b in range(4):
-                span = slice(b * toks, (b + 1) * toks)
-                dsend[l, u, span, :] = jnp.dot(act[span, :], weights,
-                                               preferred_element_type=F32).astype(BF16)
-            swaps.append(message(dsend.at[l, u], drecv.at[l, u], core_dev))
+            for m, pair in enumerate(((near, diag), (far, q))):
+                for k, b in enumerate(pair):
+                    dsend[l, u, m, k] = jnp.dot(act[block_rows(b), :], weights,
+                                                preferred_element_type=F32).astype(BF16)
+                swaps[u, m] = message(dsend.at[l, u, m], drecv.at[l, u, m], core_dev)
 
         def stage_first(u):
             weights = wo[l, :, out_cols(c, u)]
-            swaps[u].wait()
-
-            def partial(b):
+
+            def partial(b, m, k):
                 return (jnp.dot(act[block_rows(b), :], weights, preferred_element_type=F32)
-                        + drecv[l, u, block_rows(b), :].astype(F32))
-
-            asend[l, u, 0] = partial(far).astype(BF16)
-            asend[l, u, 1] = partial(diag).astype(BF16)
-            firsts.append(message(asend.at[l, u], arecv.at[l, u], far_dev))
-            through[u] = partial(near)
-            mine[u] = partial(q) + source[:, out_cols(c, u)].astype(F32)
-
-        def stage_second(u):
-            firsts[u].wait()
-            bsend[l, u] = (through[u] + arecv[l, u, 1].astype(F32)).astype(BF16)
-            seconds.append(message(bsend.at[l, u], brecv.at[l, u], near_dev))
-            mine[u] = mine[u] + arecv[l, u, 0].astype(F32)
-
-        def stage_last(u):
-            seconds[u].wait()
-            strm[l, :, out_cols(c, u)] = (mine[u] + brecv[l, u].astype(F32)).astype(BF16)
-            piece = strm.at[l, :, out_cols(c, u)]
-            lasts.append(message(piece, piece, core_dev))
+                        + drecv[l, u, m, k].astype(F32))
+
+            swaps[u, 0].wait()
+            for k, b in enumerate((far, diag)):
+                term = partial(b, 0, k).astype(BF16)
+                for j in range(2):
+                    asend[l, u, j, k] = term[j * unit:(j + 1) * unit]
+            for j in range(2):
+                firsts[u, j] = message(asend.at[l, u, j], arecv.at[l, u, j], far_dev)
+            swaps[u, 1].wait()
+            through[u] = partial(near, 1, 0)
+            mine[u] = partial(q, 1, 1) + source[:, out_cols(c, u)].astype(F32)
+
+        def stage_second(u, j):
+            span = slice(j * unit, (j + 1) * unit)
+            firsts[u, j].wait()
+            bsend[l, u, j] = (through[u, span] + arecv[l, u, j, 1].astype(F32)).astype(BF16)
+            seconds[u, j] = message(bsend.at[l, u, j], brecv.at[l, u, j], near_dev)
+            mine[u, span] = mine[u, span] + arecv[l, u, j, 0].astype(F32)
+
+        def stage_last(u, j):
+            span = slice(j * unit, (j + 1) * unit)
+            seconds[u, j].wait()
+            strm[l, span, out_cols(c, u)] = (mine[u, span] + brecv[l, u, j].astype(F32)).astype(BF16)
+            piece = strm.at[l, span, out_cols(c, u)]
+            lasts[u, j] = message(piece, piece, core_dev)
             if last_layer:
-                outs.append(pltpu.make_async_copy(piece, out.at[:, out_cols(c, u)], out_sem.at[0, u]))
-                outs[-1].start()
-
-        def finish(u):
-            lasts[u].wait()
+                write(u, j, c)
+
+        def write(u, j, h):
+            span = slice(j * unit, (j + 1) * unit)
+            pltpu.make_async_copy(strm.at[l, span, out_cols(h, u)], out.at[span, out_cols(h, u)],
+                                  out_sem.at[0]).start()
+
+        def finish(u, j):
+            lasts[u, j].wait()
             if last_layer:
-                outs.append(pltpu.make_async_copy(
-                    strm.at[l, :, out_cols(1 - c, u)], out.at[:, out_cols(1 - c, u)], out_sem.at[1, u]))
-                outs[-1].start()
-
+                write(u, j, 1 - c)
+
+        swaps, firsts, seconds, lasts = {}, {}, {}, {}
         lag = 4
         for i in range(planes + lag + 1):
             if i < planes:
                 stage_swap(i)
             if 1 <= i <= planes:
                 stage_first(i - 1)
-            if 0 <= i - lag < planes:
-                stage_second(i - lag)
-            if 0 <= i - lag - 1 < planes:
-                stage_last(i - lag - 1)
-            if not last_layer and i == 1:
+            for j in range(2):
+                if 0 <= i - lag < planes:
+                    stage_second(i - lag, j)
+                if 0 <= i - lag - 1 < planes:
+                    stage_last(i - lag - 1, j)
+            if not last_layer and i == lag + 2:
                 pump(l + 1, 0, 1)
-            if not last_layer and i == 6:
-                for t in range(2, planes - 1):
-                    pump(l + 1, 0, t)
-                pump(l + 1, 1, 0)
             if last_layer and i == planes:
                 drain(l, 0)
                 drain(l, 1)
         for u in range(planes):
-            finish(u)
-
-    for copy in outs:
-        copy.wait()
+            for j in range(2):
+                finish(u, j)
+
+    pltpu.make_async_copy(strm.at[layers - 1], out, out_sem.at[0]).wait()
 
 
 def fused(n, layers):
@@ -458,7 +505,7 @@
         chunk = 2 * rows
         taps = jnp.transpose(conv_taps, (1, 0, 2))
         hbm = pl.BlockSpec(memory_space=pltpu.HBM)
-        msgs = layers * (12 + 7 * PARTS + 4 * planes)
+        msgs = 12 + 7 * PARTS + 8 * planes
         return pl.pallas_call(
             functools.partial(kernel, n, layers, taps_n),
             out_shape=jax.ShapeDtypeStruct((toks, width), BF16),
@@ -475,24 +522,26 @@
                 pltpu.VMEM((PAD + group, ch), F32),
                 pltpu.VMEM((group, ch), F32),
                 pltpu.VMEM((group, ch), BF16),
-                pltpu.VMEM((layers, PARTS, 8, group // PARTS), F32),
-                pltpu.VMEM((layers, PARTS, 7, 8, group // PARTS), F32),
-                pltpu.VMEM((layers, planes, group, chunk), BF16),
-                pltpu.VMEM((layers, planes, group, chunk), BF16),
-                pltpu.VMEM((layers, planes, 2, toks, chunk), BF16),
-                pltpu.VMEM((layers, planes, 2, toks, chunk), BF16),
-                pltpu.VMEM((layers, planes, toks, chunk), BF16),
-                pltpu.VMEM((layers, planes, toks, chunk), BF16),
+                pltpu.VMEM((layers, PARTS, 2, group // PARTS), F32),
+                pltpu.VMEM((layers, PARTS, 7, 2, group // PARTS), F32),
+                pltpu.VMEM((layers, planes, 2, 2, toks, chunk), BF16),
+                pltpu.VMEM((layers, planes, 2, 2, toks, chunk), BF16),
+                pltpu.VMEM((layers, planes, 2, 2, toks // 2, chunk), BF16),
+                pltpu.VMEM((layers, planes, 2, 2, toks // 2, chunk), BF16),
+                pltpu.VMEM((layers, planes, 2, toks // 2, chunk), BF16),
+                pltpu.VMEM((layers, planes, 2, toks // 2, chunk), BF16),
                 pltpu.VMEM((planes, toks, chunk), F32),
                 pltpu.VMEM((planes, toks, chunk), F32),
                 pltpu.VMEM((layers, toks, width), BF16),
+                pltpu.VMEM((PAD + group, 2 * ch), F32),
+                pltpu.VMEM((128, group // PARTS), F32),
                 pltpu.SemaphoreType.DMA((4,)),
-                pltpu.SemaphoreType.DMA((2, planes)),
+                pltpu.SemaphoreType.DMA((1,)),
                 pltpu.SemaphoreType.DMA((layers * 3,)),
-                pltpu.SemaphoreType.DMA((layers * 3, 4)),
-                pltpu.SemaphoreType.DMA((layers * 3, 4)),
+                pltpu.SemaphoreType.DMA((layers * 3, 3)),
+                pltpu.SemaphoreType.DMA((layers * 3, 3)),
                 pltpu.SemaphoreType.DMA((layers * 4, planes - 1)),
-                pltpu.SemaphoreType.DMA((layers * 4, planes - 1, 4)),
+                pltpu.SemaphoreType.DMA((2 * (planes - 1) * (4 * layers + 2),)),
                 pltpu.SemaphoreType.DMA((layers, 5)),
                 pltpu.SemaphoreType.DMA((layers, 3)),
                 pltpu.SemaphoreType.DMA((msgs,)),

time: 146 us -> 139 us (0.952)
  Pallas kernels: 142 us -> 136 us
    pallas_call x1, Pallas kernels: 142 us -> 136 us  [body(): pl.pallas_call(functools.partial(kernel, n, layers, taps_n), out_shape=ja...]
where the time goes in v3:
time: 139 us
  Pallas kernels  136 us (98%)
  local copies, waits for them, and re-layouts  2.3 us (2%)
    pallas_call x1, Pallas kernels, body(): pl.pallas_call(functools.partial(kernel, n, layers, taps_n), out_shape=ja...  136 us

profile of v3, /device:TPU:0, one launch (start us, length us, event | category | flops | bytes accessed | tf_op | source)
XLA Modules:
  0.0 138.6 jit_solution(10815220887686306573)
XLA Ops:
  0.0 136.2 %shard_map.73 = bf16[256,2048]{1,0:T(8,128)(2,1)} custom-call(bf16[256,2048]{1,0:T(8,128)(2,1)} %stream_hbm.1, f32[2,2048]{1,0:T(2,128)} %gain_hbm.1, bf16[2,128,1024]{2,1,0:T(8,128)(2,1)} %vw.1, bf16[2,128,1024]{2,1,0:T(8,128)(2,1)} %gw.1, f32[31,2,1024]{2,1,0:T(2,128)} %bitcast.1, f32[2,1024]{1,0:T(2,128)} %cgain_hbm.1, bf16[2,1024,128]{2,1,0:T(8,128)(2,1)} %ow.1), custom_call_target="tpu_custom_call" | custom-call | tf_op jit(solution)/shard_map/pallas_call | solution.py:509
  136.2 2.3 %copy.9 = bf16[256,2048]{1,0:T(8,128)(2,1)} copy(bf16[256,2048]{1,0:T(8,128)(2,1)} %shard_map.73) | data formatting | bytes 2097152

commit v4 on v3

--- a/solution.py
+++ b/solution.py
@@ -18,6 +18,7 @@
 def kernel(n, layers, taps_n, stream_hbm, gain_hbm, vw, gw, taps_hbm, cgain_hbm, ow, out,
            stream_in, gain, taps, cgain, wvg, wo, nrm, gat, fil, act, ssend, srecv, dsend, drecv,
            asend, arecv, bsend, brecv, mine, through, strm, acc, turn,
+           squares, qsend, qrecv, edge_out, edge_in,
            in_sem, out_sem, loc_sem, wx_send, wx_recv, z_send, z_recv, halo_send, halo_recv,
            msg_send, msg_recv):
     planes = n // 4
@@ -107,7 +108,7 @@
             device_id=up_dev if d == 0 else down_dev, device_id_type=MESH)
 
     def pieces(l, grp):
-        return 4 if (l, grp) == (0, 0) else 2
+        return 4 if l == 0 else 2
 
     def first_recv(l, grp):
         return 2 * (planes - 1) * sum(pieces(*divmod(i, 2)) for i in range(l * 2 + grp))
@@ -118,13 +119,13 @@
     def sends(d):
         return z < planes - 1 if d == 0 else z > 0
 
-    def pump(l, grp, t):
+    def pump(l, grp, t, ks=None):
         kinds = (0, 1) if grp == 0 else (2,)
         if t == 0 and pieces(l, grp) == 2:
             for k in range(4):
                 for kind in kinds:
                     shared[l, kind, k].wait()
-        for k in range(pieces(l, grp)):
+        for k in ks or range(pieces(l, grp)):
             if t == 0 and pieces(l, grp) == 4:
                 for kind in kinds:
                     shared[l, kind, k].wait()
@@ -155,16 +156,12 @@
                     z_copy(l, grp, d, t, t, -1).wait_send()
 
     turn[...] = jnp.zeros_like(turn)
-    slots = [0]
-
-    def make(src, dst, dev):
-        slot = slots[0]
-        slots[0] += 1
-        return pltpu.make_async_remote_copy(src, dst, msg_send.at[slot], msg_recv.at[slot],
-                                            device_id=dev, device_id_type=MESH)
-
-    def message(src, dst, dev):
-        m = make(src, dst, dev)
+    slots = {}
+
+    def message(name, src, dst, dev):
+        slot = slots.setdefault(name, len(slots))
+        m = pltpu.make_async_remote_copy(src, dst, msg_send.at[slot], msg_recv.at[slot],
+                                         device_id=dev, device_id_type=MESH)
         m.start()
         return m
 
@@ -190,112 +187,107 @@
         high = planes - 1 - jnp.where(u <= zm, zm - u, u)
         return jnp.where(2 * z < planes, low, high)
 
+    def norm_step(r, _):
+        at = al(r * 64, 64)
+        wide = stream_in[pl.ds(at, 64), :].astype(F32)
+        scale = lax.rsqrt(jnp.mean(wide * wide, axis=1, keepdims=True) + epsilon)
+        nrm[0, pl.ds(al(PAD + q * toks + at, 32), 64), :] = (
+            wide * scale * gain[0:1, :]).astype(BF16)
+        return 0
+
+    class Halo:
+        def __init__(self, l, border, first):
+            def copy(k, dev, src, recv):
+                return pltpu.make_async_remote_copy(
+                    src, first, halo_send.at[l, k], halo_recv.at[l, recv],
+                    device_id=dev, device_id_type=MESH)
+
+            self.up = copy(0, up_dev, border, 0)
+            self.side = [copy(k, (z * 4 + quad[k], c), first, 1) for k in (1, 2, 3)]
+            self.core = copy(4, core_dev, first, 2)
+
+        def rise(self):
+            @pl.when((q == 3) & (z < planes - 1))
+            def _():
+                self.up.start()
+
+        def spread(self):
+            @pl.when((q == 3) & (z > 0))
+            def _():
+                self.up.wait_recv()
+                for m in self.side:
+                    m.start()
+                self.core.start()
+
+        def swap(self):
+            @pl.when((q != 3) & (z > 0))
+            def _():
+                self.side[0].wait_recv()
+                self.core.start()
+
+        def finish(self):
+            @pl.when(z > 0)
+            def _():
+                self.core.wait()
+
+            @pl.when((q == 3) & (z > 0))
+            def _():
+                for m in self.side:
+                    m.wait_send()
+
+            @pl.when((q == 3) & (z < planes - 1))
+            def _():
+                self.up.wait_send()
+
+    def spot(b, j):
+        return nrm.at[0, pl.ds(al(PAD + b * toks + j * unit, 32), unit), half_cols(c)]
+
+    def to_far(j):
+        own_near[j].wait_send()
+        own_far.append(message(("far", j), spot(q, j), spot(q, j), far_dev))
+
+    def pass_on(j):
+        own_near[j].wait_recv()
+        passed.append(message(("pass", j), spot(near, j), spot(near, j), far_dev))
+        relays[1, j] = message(("core", 1, j), spot(near, j), spot(near, j), core_dev)
+
+    def relay(which, j):
+        (own_far if which == 2 else passed)[j].wait()
+        b = far if which == 2 else diag
+        relays[which, j] = message(("core", which, j), spot(b, j), spot(b, j), core_dev)
+
+    def gate_part(l, t, plane, start, count, size):
+        depth = pl.ds(al(plane * 4 * rows, 4 * rows), 4 * rows)
+
+        def gate_step(r, _):
+            at = pl.ds(al(start + r * size, 16), size)
+            term = jnp.dot(nrm[l, at, depth], wvg[l, depth, :], preferred_element_type=F32)
+            acc[at, :] = term if t == 0 else acc[at, :] + term
+            return 0
+
+        lax.fori_loop(0, count // size, gate_step, 0)
+
     for l in range(layers):
         last_layer = l + 1 == layers
-        slots[0] = 0
         source = stream_in if l == 0 else strm.at[l - 1]
 
-        def norm_step(r, _):
-            at = al(r * 64, 64)
-            wide = source[pl.ds(at, 64), :].astype(F32)
-            scale = lax.rsqrt(jnp.mean(wide * wide, axis=1, keepdims=True) + epsilon)
-            nrm[l, pl.ds(al(PAD + q * toks + at, 32), 64), :] = (
-                wide * scale * gain[l:l + 1, :]).astype(BF16)
-            return 0
-
-        lax.fori_loop(0, toks // 64, norm_step, 0)
-
-        @pl.when(z == 0)
-        def _():
-            nrm[l, 0:PAD, :] = jnp.zeros((PAD, width), BF16)
-
-        def spot(b, j):
-            return nrm.at[l, pl.ds(al(PAD + b * toks + j * unit, 32), unit), half_cols(c)]
-
-        border = nrm.at[l, pl.ds(group, PAD), half_cols(c)]
-        first = nrm.at[l, pl.ds(0, PAD), half_cols(c)]
-
-        def halo_copy(k, dev, src, recv):
-            return pltpu.make_async_remote_copy(
-                src, first, halo_send.at[l, k], halo_recv.at[l, recv],
-                device_id=dev, device_id_type=MESH)
-
-        rise = halo_copy(0, up_dev, border, 0)
-        spread = [halo_copy(k, (z * 4 + quad[k], c), first, 1) for k in (1, 2, 3)]
-        swap_halo = halo_copy(4, core_dev, first, 2)
-
-        @pl.when((q == 3) & (z < planes - 1))
-        def _():
-            rise.start()
-
-        def halo_spread():
-            @pl.when((q == 3) & (z > 0))
-            def _():
-                rise.wait_recv()
-                for m in spread:
-                    m.start()
-                swap_halo.start()
-
-        def halo_swap():
-            @pl.when((q != 3) & (z > 0))
-            def _():
-                spread[0].wait_recv()
-                swap_halo.start()
-
-        def halo_finish():
-            @pl.when(z > 0)
-            def _():
-                swap_halo.wait()
-
-            @pl.when((q == 3) & (z > 0))
-            def _():
-                for m in spread:
-                    m.wait_send()
-
-            @pl.when((q == 3) & (z < planes - 1))
-            def _():
-                rise.wait_send()
-
-        own_near = [message(spot(q, j), spot(q, j), near_dev) for j in range(2)]
-        passed, relays, own_far = [], {}, []
-
-        def to_far(j):
-            own_near[j].wait_send()
-            own_far.append(message(spot(q, j), spot(q, j), far_dev))
-
-        def pass_on(j):
-            own_near[j].wait_recv()
-            passed.append(message(spot(near, j), spot(near, j), far_dev))
-            relays[1, j] = message(spot(near, j), spot(near, j), core_dev)
-
-        def relay(which, j):
-            (own_far if which == 2 else passed)[j].wait()
-            b = far if which == 2 else diag
-            relays[which, j] = message(spot(b, j), spot(b, j), core_dev)
-
-        def gate_rows(at, size):
-            both = jnp.dot(nrm[l, pl.ds(at, size), :], wvg[l], preferred_element_type=F32)
-            gated = (both[:, :ch] * jax.nn.sigmoid(both[:, ch:])).astype(BF16)
-            gat[pl.ds(at, size), :] = gated.astype(F32)
-
-        def gate_part(t, plane):
-            depth = pl.ds(al(plane * 4 * rows, 4 * rows), 4 * rows)
-
-            def gate_step(r, _):
-                at = pl.ds(al(r * tile, 16), tile)
-                term = jnp.dot(nrm[l, at, depth], wvg[l, depth, :], preferred_element_type=F32)
-                acc[at, :] = term if t == 0 else acc[at, :] + term
-                return 0
-
-            lax.fori_loop(0, total_rows // tile, gate_step, 0)
-
-        def gate_pair(which, j):
-            b = (q, near, far, diag)[which]
-            gate_rows(al(PAD + b * toks + j * unit, 32), unit)
-
         if l == 0:
-            pump(0, 0, 0)
-            halo_spread()
+            lax.fori_loop(0, toks // 64, norm_step, 0)
+
+            @pl.when(z == 0)
+            def _():
+                for ll in range(layers):
+                    nrm[ll, 0:PAD, :] = jnp.zeros((PAD, width), BF16)
+
+            edge = Halo(0, nrm.at[0, pl.ds(group, PAD), half_cols(c)],
+                        nrm.at[0, pl.ds(0, PAD), half_cols(c)])
+            edge.rise()
+            own_near = [message(("near", j), spot(q, j), spot(q, j), near_dev) for j in range(2)]
+            passed, relays, own_far = [], {}, []
+            pump(0, 0, 0, (0,))
+            pump(0, 1, 0, (0,))
+            pump(0, 0, 0, (1, 2, 3))
+            edge.spread()
             to_far(0)
             to_far(1)
             pump(0, 0, 1)
@@ -310,18 +302,18 @@
             relay(3, 1)
             for ll in range(1, layers):
                 share(ll, (0, 1, 2))
-            pump(0, 1, 0)
-            halo_swap()
+            pump(0, 1, 0, (1, 2, 3))
+            edge.swap()
             for m in relays.values():
                 m.wait()
-            halo_finish()
-            gate_part(0, z)
+            edge.finish()
+            gate_part(0, 0, z, 0, total_rows, tile)
             for t in range(1, planes):
                 for d in range(2):
                     @pl.when(holds(d, t))
                     def _(t=t, d=d):
                         consume_one(0, 0, t, d)
-                        gate_part(t, z - t if d == 0 else z + t)
+                        gate_part(0, t, z - t if d == 0 else z + t, 0, total_rows, tile)
 
             def gate_end(r, _):
                 at = pl.ds(al(r * tile, 16), tile)
@@ -331,40 +323,6 @@
 
             lax.fori_loop(0, total_rows // tile, gate_end, 0)
             pump(0, 1, 1)
-        else:
-            for t in range(2, planes - 1):
-                pump(l, 0, t)
-            halo_spread()
-            to_far(0)
-            to_far(1)
-            pump(l, 1, 0)
-            pass_on(0)
-            pass_on(1)
-            for t in range(1, planes):
-                consume(l, 0, t)
-            gate_pair(0, 0)
-            gate_pair(0, 1)
-            for j in range(2):
-                relay(2, j)
-                relays[1, j].wait()
-                gate_pair(2, j)
-            drain(l - 1, 0)
-            pump(l, 1, 1)
-            relay(3, 0)
-            relays[2, 0].wait()
-            gate_pair(1, 0)
-            relay(3, 1)
-            halo_swap()
-            relays[2, 1].wait()
-            gate_pair(1, 1)
-            for j in range(2):
-                relays[3, j].wait()
-                gate_pair(3, j)
-            for t in range(2, planes - 1):
-                pump(l, 1, t)
-            halo_finish()
-            gate_rows(0, PAD)
-            drain(l - 1, 1)
 
         lead = PAD - (taps_n - 1)
         step_rows = 64
@@ -394,11 +352,10 @@
             lane_id = lax.broadcasted_iota(jnp.int32, (part_rows, lanes), 1)
             stat = jnp.where(lane_id == 0, first_sum, jnp.where(lane_id == 1, second_sum, 0.0))
             ssend[l, part] = jnp.transpose(stat)[0:2, :]
-            sums.append([message(ssend.at[l, part], srecv.at[l, part, k], dev)
+            sums.append([message(("sum", part, k), ssend.at[l, part], srecv.at[l, part, k], dev)
                          for k, dev in enumerate(plane_devs)])
-        if l == 0:
-            for t in range(2, planes - 1):
-                pump(l, 1, t)
+        for t in range(2, planes - 1):
+            pump(l, 1, t)
         if not last_layer:
             pump(l + 1, 0, 0)
         for part in range(PARTS):
@@ -408,8 +365,8 @@
             whole = ssend[l, part]
             for k in range(len(plane_devs)):
                 whole = whole + srecv[l, part, k]
-            turn[0:2, :] = whole
-            stat = jnp.transpose(turn[...])
+            turn[0:2, 0:part_rows] = whole
+            stat = jnp.transpose(turn[:, 0:part_rows])
             mean_value = stat[:, 0:1] / width
             variance = stat[:, 1:2] / width - mean_value * mean_value
             act[span, :] = jax.nn.silu((fil[span, :] - mean_value) * lax.rsqrt(variance + epsilon)
@@ -426,7 +383,7 @@
                 for k, b in enumerate(pair):
                     dsend[l, u, m, k] = jnp.dot(act[block_rows(b), :], weights,
                                                 preferred_element_type=F32).astype(BF16)
-                swaps[u, m] = message(dsend.at[l, u, m], drecv.at[l, u, m], core_dev)
+                swaps[u, m] = message(("swap", u, m), dsend.at[l, u, m], drecv.at[l, u, m], core_dev)
 
         def stage_first(u):
             weights = wo[l, :, out_cols(c, u)]
@@ -441,7 +398,7 @@
                 for j in range(2):
                     asend[l, u, j, k] = term[j * unit:(j + 1) * unit]
             for j in range(2):
-                firsts[u, j] = message(asend.at[l, u, j], arecv.at[l, u, j], far_dev)
+                firsts[u, j] = message(("first", u, j), asend.at[l, u, j], arecv.at[l, u, j], far_dev)
             swaps[u, 1].wait()
             through[u] = partial(near, 1, 0)
             mine[u] = partial(q, 1, 1) + source[:, out_cols(c, u)].astype(F32)
@@ -450,17 +407,25 @@
             span = slice(j * unit, (j + 1) * unit)
             firsts[u, j].wait()
             bsend[l, u, j] = (through[u, span] + arecv[l, u, j, 1].astype(F32)).astype(BF16)
-            seconds[u, j] = message(bsend.at[l, u, j], brecv.at[l, u, j], near_dev)
+            seconds[u, j] = message(("second", u, j), bsend.at[l, u, j], brecv.at[l, u, j], near_dev)
             mine[u, span] = mine[u, span] + arecv[l, u, j, 0].astype(F32)
 
         def stage_last(u, j):
             span = slice(j * unit, (j + 1) * unit)
             seconds[u, j].wait()
-            strm[l, span, out_cols(c, u)] = (mine[u, span] + brecv[l, u, j].astype(F32)).astype(BF16)
-            piece = strm.at[l, span, out_cols(c, u)]
-            lasts[u, j] = message(piece, piece, core_dev)
+            final = (mine[u, span] + brecv[l, u, j].astype(F32)).astype(BF16)
+            strm[l, span, out_cols(c, u)] = final
             if last_layer:
+                piece = strm.at[l, span, out_cols(c, u)]
+                lasts[u, j] = message(("last", u, j), piece, piece, core_dev)
                 write(u, j, c)
+            else:
+                wide = final.astype(F32)
+                nrm[l + 1, pl.ds(al(PAD + q * toks + j * unit, 32), unit), out_cols(c, u)] = (
+                    wide * gain[l + 1:l + 2, out_cols(c, u)]).astype(BF16)
+                square = wide * wide
+                folded = sum(square[:, k * lanes:(k + 1) * lanes] for k in range(chunk // lanes))
+                squares[span, :] = folded if u == 0 else squares[span, :] + folded
 
         def write(u, j, h):
             span = slice(j * unit, (j + 1) * unit)
@@ -469,10 +434,81 @@
 
         def finish(u, j):
             lasts[u, j].wait()
-            if last_layer:
-                write(u, j, 1 - c)
-
-        swaps, firsts, seconds, lasts = {}, {}, {}, {}
+            write(u, j, 1 - c)
+
+        def lot(b, u):
+            return nrm.at[l + 1, pl.ds(al(PAD + b * toks, 32), toks), out_cols(c, u)]
+
+        def pass_chunk(kind, u, b, dev):
+            moves[kind, u] = message((kind, u), lot(b, u), lot(b, u), dev)
+
+        def gather(u):
+            pass_chunk("g_near", u, q, near_dev)
+            pass_chunk("g_far", u, q, far_dev)
+            pass_chunk("c_own", u, q, core_dev)
+
+        def forward(u):
+            moves["g_near", u].wait()
+            pass_chunk("g_pass", u, near, far_dev)
+            pass_chunk("c_near", u, near, core_dev)
+
+        def cross_far(u):
+            moves["g_far", u].wait()
+            pass_chunk("c_far", u, far, core_dev)
+
+        def cross_diag(u):
+            moves["g_pass", u].wait()
+            pass_chunk("c_diag", u, diag, core_dev)
+
+        def gate_chunk(u):
+            if u > 0:
+                consume(l + 1, 0, u)
+            for kind in ("c_own", "c_near", "c_far", "c_diag"):
+                moves[kind, u].wait()
+            gate_part(l + 1, u, plane_at(u), PAD, group, toks)
+
+        def send_squares():
+            lane_id = lax.broadcasted_iota(jnp.int32, (toks, lanes), 1)
+            total = jnp.sum(squares[...], axis=1, keepdims=True)
+            qsend[l] = jnp.transpose(jnp.where(lane_id == 0, total, 0.0))[0:2, :]
+            return [message(("square", k), qsend.at[l], qrecv.at[l, k], dev)
+                    for k, dev in enumerate(plane_devs)]
+
+        def row_scale(whole):
+            turn[0:2, 0:toks] = whole
+            return lax.rsqrt(jnp.transpose(turn[:, 0:toks])[:, 0:1] / width + epsilon)
+
+        def send_edge(edge):
+            norms[0].wait()
+            scale = row_scale(qsend[l] + qrecv[l, 0])[toks - PAD:]
+            for u in range(planes):
+                edge_out[l, :, pl.ds(al(plane_at(u) * chunk, chunk), chunk)] = (
+                    strm[l, toks - PAD:, out_cols(c, u)].astype(F32) * scale
+                    * gain[l + 1:l + 2, out_cols(c, u)]).astype(BF16)
+            edge.rise()
+
+        def gate_final(edge):
+            edge.finish()
+
+            @pl.when(z > 0)
+            def _():
+                for p in range(planes):
+                    for h in range(2):
+                        at = p * 4 * rows + h * chunk
+                        nrm[l + 1, 0:PAD, at:at + chunk] = edge_in[l, h, :, p * chunk:(p + 1) * chunk]
+
+            both = jnp.dot(nrm[l + 1, 0:PAD, :], wvg[l + 1], preferred_element_type=F32)
+            gat[0:PAD, :] = (both[:, :ch] * jax.nn.sigmoid(both[:, ch:])).astype(BF16).astype(F32)
+            for m in norms[1:]:
+                m.wait()
+            for k in range(4):
+                mate = qsend[l] if k == 0 else qrecv[l, 2 * k - 1]
+                scale = row_scale(mate + qrecv[l, 2 * k])
+                at = pl.ds(al(PAD + quad[k] * toks, 32), toks)
+                value, gate = acc[at, :ch] * scale, acc[at, ch:] * scale
+                gat[at, :] = (value * jax.nn.sigmoid(gate)).astype(BF16).astype(F32)
+
+        swaps, firsts, seconds, lasts, moves = {}, {}, {}, {}, {}
         lag = 4
         for i in range(planes + lag + 1):
             if i < planes:
@@ -484,14 +520,46 @@
                     stage_second(i - lag, j)
                 if 0 <= i - lag - 1 < planes:
                     stage_last(i - lag - 1, j)
-            if not last_layer and i == lag + 2:
-                pump(l + 1, 0, 1)
+            if not last_layer:
+                if i - lag - 1 >= 0:
+                    gather(i - lag - 1)
+                if i - lag - 3 >= 0:
+                    forward(i - lag - 3)
+                if i == lag + 2:
+                    pump(l + 1, 0, 1)
             if last_layer and i == planes:
                 drain(l, 0)
                 drain(l, 1)
-        for u in range(planes):
-            for j in range(2):
-                finish(u, j)
+        if last_layer:
+            for u in range(planes):
+                for j in range(2):
+                    finish(u, j)
+        else:
+            edge = Halo(l + 1, edge_out.at[l], edge_in.at[l, c])
+            norms = send_squares()
+            cross_far(0)
+            send_edge(edge)
+            ahead = planes - 2
+            for u in range(ahead, planes + ahead):
+                if u < planes:
+                    forward(u)
+                    cross_far(u - ahead + 1)
+                elif u - ahead + 1 < planes:
+                    cross_far(u - ahead + 1)
+                cross_diag(u - ahead)
+                if u == ahead:
+                    for t in range(2, planes - 1):
+                        pump(l + 1, 0, t)
+                if u == ahead + 1:
+                    edge.spread()
+                    pump(l + 1, 1, 0)
+                gate_chunk(u - ahead)
+                if u == ahead + 2:
+                    drain(l, 0)
+                    drain(l, 1)
+            edge.swap()
+            gate_final(edge)
+            pump(l + 1, 1, 1)
 
     pltpu.make_async_copy(strm.at[layers - 1], out, out_sem.at[0]).wait()
 
@@ -505,7 +573,7 @@
         chunk = 2 * rows
         taps = jnp.transpose(conv_taps, (1, 0, 2))
         hbm = pl.BlockSpec(memory_space=pltpu.HBM)
-        msgs = 12 + 7 * PARTS + 8 * planes
+        msgs = 12 + 7 + 7 * PARTS + 15 * planes
         return pl.pallas_call(
             functools.partial(kernel, n, layers, taps_n),
             out_shape=jax.ShapeDtypeStruct((toks, width), BF16),
@@ -534,14 +602,19 @@
                 pltpu.VMEM((planes, toks, chunk), F32),
                 pltpu.VMEM((layers, toks, width), BF16),
                 pltpu.VMEM((PAD + group, 2 * ch), F32),
-                pltpu.VMEM((128, group // PARTS), F32),
+                pltpu.VMEM((128, group), F32),
+                pltpu.VMEM((toks, 128), F32),
+                pltpu.VMEM((layers, 2, toks), F32),
+                pltpu.VMEM((layers, 7, 2, toks), F32),
+                pltpu.VMEM((layers, PAD, half), BF16),
+                pltpu.VMEM((layers, 2, PAD, half), BF16),
                 pltpu.SemaphoreType.DMA((4,)),
                 pltpu.SemaphoreType.DMA((1,)),
                 pltpu.SemaphoreType.DMA((layers * 3,)),
                 pltpu.SemaphoreType.DMA((layers * 3, 3)),
                 pltpu.SemaphoreType.DMA((layers * 3, 3)),
                 pltpu.SemaphoreType.DMA((layers * 4, planes - 1)),
-                pltpu.SemaphoreType.DMA((2 * (planes - 1) * (4 * layers + 2),)),
+                pltpu.SemaphoreType.DMA((2 * (planes - 1) * (4 * layers + 4),)),
                 pltpu.SemaphoreType.DMA((layers, 5)),
                 pltpu.SemaphoreType.DMA((layers, 3)),
                 pltpu.SemaphoreType.DMA((msgs,)),

time: 139 us -> 134 us (0.964)
  Pallas kernels: 136 us -> 132 us
    pallas_call x1, Pallas kernels: 136 us -> 132 us  [body(): pl.pallas_call(functools.partial(kernel, n, layers, taps_n), out_shape=ja...]
where the time goes in v4:
time: 134 us
  Pallas kernels  132 us (99%)
  local copies, waits for them, and re-layouts  2.3 us (2%)
    pallas_call x1, Pallas kernels, body(): pl.pallas_call(functools.partial(kernel, n, layers, taps_n), out_shape=ja...  132 us

profile of v4, /device:TPU:0, one launch (start us, length us, event | category | flops | bytes accessed | tf_op | source)
XLA Modules:
  0.0 134.2 jit_solution(16526287434012699279)
XLA Ops:
  0.0 131.9 %shard_map.73 = bf16[256,2048]{1,0:T(8,128)(2,1)} custom-call(bf16[256,2048]{1,0:T(8,128)(2,1)} %stream_hbm.1, f32[2,2048]{1,0:T(2,128)} %gain_hbm.1, bf16[2,128,1024]{2,1,0:T(8,128)(2,1)} %vw.1, bf16[2,128,1024]{2,1,0:T(8,128)(2,1)} %gw.1, f32[31,2,1024]{2,1,0:T(2,128)} %bitcast.1, f32[2,1024]{1,0:T(2,128)} %cgain_hbm.1, bf16[2,1024,128]{2,1,0:T(8,128)(2,1)} %ow.1), custom_call_target="tpu_custom_call" | custom-call | tf_op jit(solution)/shard_map/pallas_call | solution.py:577
  131.9 2.3 %copy.9 = bf16[256,2048]{1,0:T(8,128)(2,1)} copy(bf16[256,2048]{1,0:T(8,128)(2,1)} %shard_map.73) | data formatting | bytes 2097152

commit v5 on v4

--- a/solution.py
+++ b/solution.py
@@ -77,7 +77,7 @@
             copy = pltpu.make_async_copy(src, dst, loc_sem.at[idx])
         else:
             copy = pltpu.make_async_remote_copy(
-                src, dst, wx_send.at[idx, k - 1], wx_recv.at[idx, k - 1],
+                src, dst, wx_send.at[0], wx_recv.at[idx, k - 1],
                 device_id=(z * 4 + quad[k], c), device_id_type=MESH)
         copy.start()
         shared[l, kind, k] = copy
@@ -93,25 +93,17 @@
     pl.semaphore_wait(barrier, len(plane_devs) + (z < planes - 1).astype(jnp.int32)
                       + (z > 0).astype(jnp.int32))
 
-    def z_copy(l, grp, d, t, hop, k):
+    def z_copy(l, grp, d, t, hop, first, count, pair):
         plane = z - t if d == 0 else z + t
-        if k < 0:
-            block = pl.ds(al(plane * 4 * rows, rows), 4 * rows)
-        elif pieces(l, grp) == 4:
-            block = pl.ds(al((plane * 4 + quad[k]) * rows, rows), rows)
-        else:
-            block = pl.ds(al((plane * 4 + 2 * k) * rows, rows), 2 * rows)
+        block = pl.ds(al((plane * 4 + first) * rows, rows), count * rows)
         ref = wvg.at[l, block, :] if grp == 0 else wo.at[l, :, block]
         idx = (l * 2 + grp) * 2 + d
         return pltpu.make_async_remote_copy(
-            ref, ref, z_send.at[idx, hop], z_recv.at[first_recv(l, grp) + (d * (planes - 1) + hop) * pieces(l, grp) + max(k, 0)],
+            ref, ref, z_send.at[idx, hop], z_recv.at[idx, hop, pair],
             device_id=up_dev if d == 0 else down_dev, device_id_type=MESH)
 
-    def pieces(l, grp):
-        return 4 if l == 0 else 2
-
-    def first_recv(l, grp):
-        return 2 * (planes - 1) * sum(pieces(*divmod(i, 2)) for i in range(l * 2 + grp))
+    def z_pair(l, grp, d, t, hop, pair):
+        return z_copy(l, grp, d, t, hop, 2 * (y + pair - 2 * y * pair), 2, pair)
 
     def holds(d, t):
         return z >= t if d == 0 else z + t < planes
@@ -119,28 +111,33 @@
     def sends(d):
         return z < planes - 1 if d == 0 else z > 0
 
-    def pump(l, grp, t, ks=None):
-        kinds = (0, 1) if grp == 0 else (2,)
-        if t == 0 and pieces(l, grp) == 2:
-            for k in range(4):
-                for kind in kinds:
-                    shared[l, kind, k].wait()
-        for k in ks or range(pieces(l, grp)):
-            if t == 0 and pieces(l, grp) == 4:
-                for kind in kinds:
-                    shared[l, kind, k].wait()
-            for d in range(2):
-                @pl.when(holds(d, t) & sends(d))
-                def _(k=k, d=d):
-                    if t > 0:
-                        z_copy(l, grp, d, t, t - 1, k).wait_recv()
-                    z_copy(l, grp, d, t, t, k).start()
+    def pump(l, grp, t, ks=(0, 1, 2, 3)):
+        if t == 0:
+            for k in ks:
+                for kind in ((0, 1) if grp == 0 else (2,)):
+                    if k:
+                        shared[l, kind, k].wait_recv()
+                    else:
+                        shared[l, kind, k].wait()
+                if l == 0:
+                    for d in range(2):
+                        @pl.when(sends(d))
+                        def _(k=k, d=d):
+                            z_copy(l, grp, d, 0, 0, quad[k], 1, k // 2).start()
+        if t > 0 or l > 0:
+            for pair in range(2):
+                for d in range(2):
+                    @pl.when(holds(d, t) & sends(d))
+                    def _(pair=pair, d=d):
+                        if t > 0:
+                            z_pair(l, grp, d, t, t - 1, pair).wait_recv()
+                        z_pair(l, grp, d, t, t, pair).start()
 
     def consume_one(l, grp, t, d):
         @pl.when(jnp.logical_not(sends(d)))
         def _():
-            for k in range(pieces(l, grp)):
-                z_copy(l, grp, d, t, t - 1, k).wait_recv()
+            for pair in range(2):
+                z_pair(l, grp, d, t, t - 1, pair).wait_recv()
 
     def consume(l, grp, t):
         for d in range(2):
@@ -153,21 +150,24 @@
             for d in range(2):
                 @pl.when(holds(d, t) & sends(d))
                 def _(t=t, d=d):
-                    z_copy(l, grp, d, t, t, -1).wait_send()
+                    z_copy(l, grp, d, t, t, 0, 4, 0).wait_send()
 
     turn[...] = jnp.zeros_like(turn)
-    slots = {}
-
-    def message(name, src, dst, dev):
+    slots, kinds_sent = {}, {}
+
+    def message(name, src, dst, dev, sender):
         slot = slots.setdefault(name, len(slots))
-        m = pltpu.make_async_remote_copy(src, dst, msg_send.at[slot], msg_recv.at[slot],
+        kind = kinds_sent.setdefault(sender, len(kinds_sent))
+        m = pltpu.make_async_remote_copy(src, dst, msg_send.at[kind], msg_recv.at[slot],
                                          device_id=dev, device_id_type=MESH)
         m.start()
         return m
 
+    def all_sent(sender, ref):
+        pltpu.make_async_remote_copy(ref, ref, msg_send.at[kinds_sent[sender]], msg_recv.at[0],
+                                     device_id=core_dev, device_id_type=MESH).wait_send()
+
     share(0, (0, 1))
-    for load in loads:
-        load.wait()
 
     def block_rows(b):
         return pl.ds(al(b * toks, toks), toks)
@@ -244,17 +244,17 @@
 
     def to_far(j):
         own_near[j].wait_send()
-        own_far.append(message(("far", j), spot(q, j), spot(q, j), far_dev))
+        own_far.append(message(("g_far", j), spot(q, j), spot(q, j), far_dev, "ag"))
 
     def pass_on(j):
         own_near[j].wait_recv()
-        passed.append(message(("pass", j), spot(near, j), spot(near, j), far_dev))
-        relays[1, j] = message(("core", 1, j), spot(near, j), spot(near, j), core_dev)
+        passed.append(message(("g_pass", j), spot(near, j), spot(near, j), far_dev, "ag"))
+        relays[1, j] = message(("c_near", j), spot(near, j), spot(near, j), core_dev, "ag")
 
     def relay(which, j):
-        (own_far if which == 2 else passed)[j].wait()
+        (own_far if which == 2 else passed)[j].wait_recv()
         b = far if which == 2 else diag
-        relays[which, j] = message(("core", which, j), spot(b, j), spot(b, j), core_dev)
+        relays[which, j] = message(("c_far" if which == 2 else "c_diag", j), spot(b, j), spot(b, j), core_dev, "ag")
 
     def gate_part(l, t, plane, start, count, size):
         depth = pl.ds(al(plane * 4 * rows, 4 * rows), 4 * rows)
@@ -272,6 +272,10 @@
         source = stream_in if l == 0 else strm.at[l - 1]
 
         if l == 0:
+            pump(0, 0, 0, (0,))
+            pump(0, 1, 0, (0,))
+            for load in loads:
+                load.wait()
             lax.fori_loop(0, toks // 64, norm_step, 0)
 
             @pl.when(z == 0)
@@ -282,10 +286,8 @@
             edge = Halo(0, nrm.at[0, pl.ds(group, PAD), half_cols(c)],
                         nrm.at[0, pl.ds(0, PAD), half_cols(c)])
             edge.rise()
-            own_near = [message(("near", j), spot(q, j), spot(q, j), near_dev) for j in range(2)]
+            own_near = [message(("g_near", j), spot(q, j), spot(q, j), near_dev, ("near", j)) for j in range(2)]
             passed, relays, own_far = [], {}, []
-            pump(0, 0, 0, (0,))
-            pump(0, 1, 0, (0,))
             pump(0, 0, 0, (1, 2, 3))
             edge.spread()
             to_far(0)
@@ -305,7 +307,7 @@
             pump(0, 1, 0, (1, 2, 3))
             edge.swap()
             for m in relays.values():
-                m.wait()
+                m.wait_recv()
             edge.finish()
             gate_part(0, 0, z, 0, total_rows, tile)
             for t in range(1, planes):
@@ -352,7 +354,7 @@
             lane_id = lax.broadcasted_iota(jnp.int32, (part_rows, lanes), 1)
             stat = jnp.where(lane_id == 0, first_sum, jnp.where(lane_id == 1, second_sum, 0.0))
             ssend[l, part] = jnp.transpose(stat)[0:2, :]
-            sums.append([message(("sum", part, k), ssend.at[l, part], srecv.at[l, part, k], dev)
+            sums.append([message(("sum", part, k), ssend.at[l, part], srecv.at[l, part, k], dev, "sum")
                          for k, dev in enumerate(plane_devs)])
         for t in range(2, planes - 1):
             pump(l, 1, t)
@@ -361,7 +363,7 @@
         for part in range(PARTS):
             span = slice(part * part_rows, (part + 1) * part_rows)
             for m in sums[part]:
-                m.wait()
+                m.wait_recv()
             whole = ssend[l, part]
             for k in range(len(plane_devs)):
                 whole = whole + srecv[l, part, k]
@@ -383,7 +385,7 @@
                 for k, b in enumerate(pair):
                     dsend[l, u, m, k] = jnp.dot(act[block_rows(b), :], weights,
                                                 preferred_element_type=F32).astype(BF16)
-                swaps[u, m] = message(("swap", u, m), dsend.at[l, u, m], drecv.at[l, u, m], core_dev)
+                swaps[u, m] = message(("swap", u, m), dsend.at[l, u, m], drecv.at[l, u, m], core_dev, "swap")
 
         def stage_first(u):
             weights = wo[l, :, out_cols(c, u)]
@@ -392,32 +394,32 @@
                 return (jnp.dot(act[block_rows(b), :], weights, preferred_element_type=F32)
                         + drecv[l, u, m, k].astype(F32))
 
-            swaps[u, 0].wait()
+            swaps[u, 0].wait_recv()
             for k, b in enumerate((far, diag)):
                 term = partial(b, 0, k).astype(BF16)
                 for j in range(2):
                     asend[l, u, j, k] = term[j * unit:(j + 1) * unit]
             for j in range(2):
-                firsts[u, j] = message(("first", u, j), asend.at[l, u, j], arecv.at[l, u, j], far_dev)
-            swaps[u, 1].wait()
+                firsts[u, j] = message(("first", u, j), asend.at[l, u, j], arecv.at[l, u, j], far_dev, "first")
+            swaps[u, 1].wait_recv()
             through[u] = partial(near, 1, 0)
             mine[u] = partial(q, 1, 1) + source[:, out_cols(c, u)].astype(F32)
 
         def stage_second(u, j):
             span = slice(j * unit, (j + 1) * unit)
-            firsts[u, j].wait()
+            firsts[u, j].wait_recv()
             bsend[l, u, j] = (through[u, span] + arecv[l, u, j, 1].astype(F32)).astype(BF16)
-            seconds[u, j] = message(("second", u, j), bsend.at[l, u, j], brecv.at[l, u, j], near_dev)
+            seconds[u, j] = message(("second", u, j), bsend.at[l, u, j], brecv.at[l, u, j], near_dev, "second")
             mine[u, span] = mine[u, span] + arecv[l, u, j, 0].astype(F32)
 
         def stage_last(u, j):
             span = slice(j * unit, (j + 1) * unit)
-            seconds[u, j].wait()
+            seconds[u, j].wait_recv()
             final = (mine[u, span] + brecv[l, u, j].astype(F32)).astype(BF16)
             strm[l, span, out_cols(c, u)] = final
             if last_layer:
                 piece = strm.at[l, span, out_cols(c, u)]
-                lasts[u, j] = message(("last", u, j), piece, piece, core_dev)
+                lasts[u, j] = message(("c_own" if j else "c_near", u), piece, piece, core_dev, "last")
                 write(u, j, c)
             else:
                 wide = final.astype(F32)
@@ -433,14 +435,14 @@
                                   out_sem.at[0]).start()
 
         def finish(u, j):
-            lasts[u, j].wait()
+            lasts[u, j].wait_recv()
             write(u, j, 1 - c)
 
         def lot(b, u):
             return nrm.at[l + 1, pl.ds(al(PAD + b * toks, 32), toks), out_cols(c, u)]
 
         def pass_chunk(kind, u, b, dev):
-            moves[kind, u] = message((kind, u), lot(b, u), lot(b, u), dev)
+            moves[kind, u] = message((kind, u), lot(b, u), lot(b, u), dev, kind[0])
 
         def gather(u):
             pass_chunk("g_near", u, q, near_dev)
@@ -448,30 +450,30 @@
             pass_chunk("c_own", u, q, core_dev)
 
         def forward(u):
-            moves["g_near", u].wait()
+            moves["g_near", u].wait_recv()
             pass_chunk("g_pass", u, near, far_dev)
             pass_chunk("c_near", u, near, core_dev)
 
         def cross_far(u):
-            moves["g_far", u].wait()
+            moves["g_far", u].wait_recv()
             pass_chunk("c_far", u, far, core_dev)
 
         def cross_diag(u):
-            moves["g_pass", u].wait()
+            moves["g_pass", u].wait_recv()
             pass_chunk("c_diag", u, diag, core_dev)
 
         def gate_chunk(u):
             if u > 0:
                 consume(l + 1, 0, u)
             for kind in ("c_own", "c_near", "c_far", "c_diag"):
-                moves[kind, u].wait()
+                moves[kind, u].wait_recv()
             gate_part(l + 1, u, plane_at(u), PAD, group, toks)
 
         def send_squares():
             lane_id = lax.broadcasted_iota(jnp.int32, (toks, lanes), 1)
             total = jnp.sum(squares[...], axis=1, keepdims=True)
             qsend[l] = jnp.transpose(jnp.where(lane_id == 0, total, 0.0))[0:2, :]
-            return [message(("square", k), qsend.at[l], qrecv.at[l, k], dev)
+            return [message(("square", k), qsend.at[l], qrecv.at[l, k], dev, "square")
                     for k, dev in enumerate(plane_devs)]
 
         def row_scale(whole):
@@ -479,7 +481,7 @@
             return lax.rsqrt(jnp.transpose(turn[:, 0:toks])[:, 0:1] / width + epsilon)
 
         def send_edge(edge):
-            norms[0].wait()
+            norms[0].wait_recv()
             scale = row_scale(qsend[l] + qrecv[l, 0])[toks - PAD:]
             for u in range(planes):
                 edge_out[l, :, pl.ds(al(plane_at(u) * chunk, chunk), chunk)] = (
@@ -500,7 +502,7 @@
             both = jnp.dot(nrm[l + 1, 0:PAD, :], wvg[l + 1], preferred_element_type=F32)
             gat[0:PAD, :] = (both[:, :ch] * jax.nn.sigmoid(both[:, ch:])).astype(BF16).astype(F32)
             for m in norms[1:]:
-                m.wait()
+                m.wait_recv()
             for k in range(4):
                 mate = qsend[l] if k == 0 else qrecv[l, 2 * k - 1]
                 scale = row_scale(mate + qrecv[l, 2 * k])
@@ -530,6 +532,15 @@
             if last_layer and i == planes:
                 drain(l, 0)
                 drain(l, 1)
+                pltpu.make_async_remote_copy(
+                    wvg.at[:, 0:9 * rows // 2, :], wvg.at[:, 0:9 * rows // 2, :], wx_send.at[0],
+                    wx_recv.at[0, 0], device_id=core_dev, device_id_type=MESH).wait_send()
+                all_sent("ag", nrm.at[0, PAD:PAD + 5 * toks // 2, :])
+                all_sent("sum", srecv)
+                if layers > 1:
+                    all_sent("square", qrecv.at[0:layers - 1])
+                    all_sent("g", nrm.at[1:layers, PAD:PAD + 3 * toks, 0:half])
+                    all_sent("c", nrm.at[1:layers, PAD:PAD + group, 0:half])
         if last_layer:
             for u in range(planes):
                 for j in range(2):
@@ -561,6 +572,10 @@
             gate_final(edge)
             pump(l + 1, 1, 1)
 
+    all_sent("swap", dsend)
+    all_sent("first", asend)
+    all_sent("second", bsend)
+    all_sent("last", strm.at[layers - 1, :, 0:half])
     pltpu.make_async_copy(strm.at[layers - 1], out, out_sem.at[0]).wait()
 
 
@@ -573,7 +588,7 @@
         chunk = 2 * rows
         taps = jnp.transpose(conv_taps, (1, 0, 2))
         hbm = pl.BlockSpec(memory_space=pltpu.HBM)
-        msgs = 12 + 7 + 7 * PARTS + 15 * planes
+        msgs = 7 + 7 * PARTS + 13 * planes
         return pl.pallas_call(
             functools.partial(kernel, n, layers, taps_n),
             out_shape=jax.ShapeDtypeStruct((toks, width), BF16),
@@ -611,13 +626,13 @@
                 pltpu.SemaphoreType.DMA((4,)),
                 pltpu.SemaphoreType.DMA((1,)),
                 pltpu.SemaphoreType.DMA((layers * 3,)),
-                pltpu.SemaphoreType.DMA((layers * 3, 3)),
+                pltpu.SemaphoreType.DMA((1,)),
                 pltpu.SemaphoreType.DMA((layers * 3, 3)),
                 pltpu.SemaphoreType.DMA((layers * 4, planes - 1)),
-                pltpu.SemaphoreType.DMA((2 * (planes - 1) * (4 * layers + 4),)),
+                pltpu.SemaphoreType.DMA((layers * 4, planes - 1, 2)),
                 pltpu.SemaphoreType.DMA((layers, 5)),
                 pltpu.SemaphoreType.DMA((layers, 3)),
-                pltpu.SemaphoreType.DMA((msgs,)),
+                pltpu.SemaphoreType.DMA((11,)),
                 pltpu.SemaphoreType.DMA((msgs,)),
             ],
             compiler_params=pltpu.CompilerParams(

time: 134 us -> 133 us (level)
  Pallas kernels: 132 us -> 130 us
    pallas_call x1, Pallas kernels: 132 us -> 130 us  [body(): pl.pallas_call(functools.partial(kernel, n, layers, taps_n), out_shape=ja...]
where the time goes in v5:
time: 133 us
  Pallas kernels  130 us (98%)
  local copies, waits for them, and re-layouts  2.3 us (2%)
    pallas_call x1, Pallas kernels, body(): pl.pallas_call(functools.partial(kernel, n, layers, taps_n), out_shape=ja...  130 us

profile of v5, /device:TPU:0, one launch (start us, length us, event | category | flops | bytes accessed | tf_op | source)
XLA Modules:
  0.0 132.5 jit_solution(18047114888131609833)
XLA Ops:
  0.0 130.2 %shard_map.73 = bf16[256,2048]{1,0:T(8,128)(2,1)} custom-call(bf16[256,2048]{1,0:T(8,128)(2,1)} %stream_hbm.1, f32[2,2048]{1,0:T(2,128)} %gain_hbm.1, bf16[2,128,1024]{2,1,0:T(8,128)(2,1)} %vw.1, bf16[2,128,1024]{2,1,0:T(8,128)(2,1)} %gw.1, f32[31,2,1024]{2,1,0:T(2,128)} %bitcast.1, f32[2,1024]{1,0:T(2,128)} %cgain_hbm.1, bf16[2,1024,128]{2,1,0:T(8,128)(2,1)} %ow.1), custom_call_target="tpu_custom_call" | custom-call | tf_op jit(solution)/shard_map/pallas_call | solution.py:592
  130.2 2.3 %copy.9 = bf16[256,2048]{1,0:T(8,128)(2,1)} copy(bf16[256,2048]{1,0:T(8,128)(2,1)} %shard_map.73) | data formatting | bytes 2097152

commit v6 on v5

--- a/solution.py
+++ b/solution.py
@@ -163,6 +163,10 @@
         m.start()
         return m
 
+    def all_came(name, ref):
+        pltpu.make_async_remote_copy(ref, ref, msg_send.at[0], msg_recv.at[slots[name]],
+                                     device_id=core_dev, device_id_type=MESH).wait_recv()
+
     def all_sent(sender, ref):
         pltpu.make_async_remote_copy(ref, ref, msg_send.at[kinds_sent[sender]], msg_recv.at[0],
                                      device_id=core_dev, device_id_type=MESH).wait_send()
@@ -178,7 +182,7 @@
     unit = toks // 2
     total_rows = PAD + group
     tile = max(v for v in range(16, 401, 16) if total_rows % v == 0)
-    part_rows = group // PARTS
+    bounds = (0, 3 * toks, group)
     lanes = 128
 
     def plane_at(u):
@@ -249,12 +253,12 @@
     def pass_on(j):
         own_near[j].wait_recv()
         passed.append(message(("g_pass", j), spot(near, j), spot(near, j), far_dev, "ag"))
-        relays[1, j] = message(("c_near", j), spot(near, j), spot(near, j), core_dev, "ag")
+        relays[1, j] = message(("c", 0), spot(near, j), spot(near, j), core_dev, "ag")
 
     def relay(which, j):
         (own_far if which == 2 else passed)[j].wait_recv()
         b = far if which == 2 else diag
-        relays[which, j] = message(("c_far" if which == 2 else "c_diag", j), spot(b, j), spot(b, j), core_dev, "ag")
+        relays[which, j] = message(("c", 0), spot(b, j), spot(b, j), core_dev, "ag")
 
     def gate_part(l, t, plane, start, count, size):
         depth = pl.ds(al(plane * 4 * rows, 4 * rows), 4 * rows)
@@ -306,8 +310,7 @@
                 share(ll, (0, 1, 2))
             pump(0, 1, 0, (1, 2, 3))
             edge.swap()
-            for m in relays.values():
-                m.wait_recv()
+            all_came(("c", 0), nrm.at[0, PAD:PAD + 3 * toks, 0:half])
             edge.finish()
             gate_part(0, 0, z, 0, total_rows, tile)
             for t in range(1, planes):
@@ -344,35 +347,34 @@
                 fil[pl.ds(at, step_rows), cut] = total
             return 0
 
-        per = part_rows // step_rows
         sums = []
         for part in range(PARTS):
-            lax.fori_loop(part * per, (part + 1) * per, conv_step, 0)
-            wide = fil[part * part_rows:(part + 1) * part_rows, :]
+            low, high = bounds[part:part + 2]
+            lax.fori_loop(low // step_rows, high // step_rows, conv_step, 0)
+            wide = fil[low:high, :]
             first_sum = jnp.sum(wide, axis=1, keepdims=True)
             second_sum = jnp.sum(wide * wide, axis=1, keepdims=True)
-            lane_id = lax.broadcasted_iota(jnp.int32, (part_rows, lanes), 1)
+            lane_id = lax.broadcasted_iota(jnp.int32, (high - low, lanes), 1)
             stat = jnp.where(lane_id == 0, first_sum, jnp.where(lane_id == 1, second_sum, 0.0))
-            ssend[l, part] = jnp.transpose(stat)[0:2, :]
-            sums.append([message(("sum", part, k), ssend.at[l, part], srecv.at[l, part, k], dev, "sum")
-                         for k, dev in enumerate(plane_devs)])
+            ssend[l, :, low:high] = jnp.transpose(stat)[0:2, :]
+            sums.append([message(("sum", part), ssend.at[l, :, low:high], srecv.at[l, k, :, low:high],
+                                 dev, "sum") for k, dev in enumerate(plane_devs)])
         for t in range(2, planes - 1):
             pump(l, 1, t)
         if not last_layer:
             pump(l + 1, 0, 0)
         for part in range(PARTS):
-            span = slice(part * part_rows, (part + 1) * part_rows)
-            for m in sums[part]:
-                m.wait_recv()
-            whole = ssend[l, part]
+            low, high = bounds[part:part + 2]
+            all_came(("sum", part), srecv.at[l, :, :, low:high])
+            whole = ssend[l, :, low:high]
             for k in range(len(plane_devs)):
-                whole = whole + srecv[l, part, k]
-            turn[0:2, 0:part_rows] = whole
-            stat = jnp.transpose(turn[:, 0:part_rows])
+                whole = whole + srecv[l, k, :, low:high]
+            turn[0:2, low:high] = whole
+            stat = jnp.transpose(turn[:, low:high])
             mean_value = stat[:, 0:1] / width
             variance = stat[:, 1:2] / width - mean_value * mean_value
-            act[span, :] = jax.nn.silu((fil[span, :] - mean_value) * lax.rsqrt(variance + epsilon)
-                                       * cgain[l:l + 1, :]).astype(BF16)
+            act[low:high, :] = jax.nn.silu((fil[low:high, :] - mean_value) * lax.rsqrt(variance + epsilon)
+                                           * cgain[l:l + 1, :]).astype(BF16)
 
         def out_cols(h, u):
             return pl.ds(al(plane_at(u) * 4 * rows + h * chunk, chunk), chunk)
@@ -405,12 +407,15 @@
             through[u] = partial(near, 1, 0)
             mine[u] = partial(q, 1, 1) + source[:, out_cols(c, u)].astype(F32)
 
-        def stage_second(u, j):
+        def stage_take(u, j):
             span = slice(j * unit, (j + 1) * unit)
             firsts[u, j].wait_recv()
             bsend[l, u, j] = (through[u, span] + arecv[l, u, j, 1].astype(F32)).astype(BF16)
-            seconds[u, j] = message(("second", u, j), bsend.at[l, u, j], brecv.at[l, u, j], near_dev, "second")
             mine[u, span] = mine[u, span] + arecv[l, u, j, 0].astype(F32)
+
+        def stage_give(u, j):
+            seconds[u, j] = message(("second", u, j), bsend.at[l, u, j], brecv.at[l, u, j], near_dev,
+                                    "second")
 
         def stage_last(u, j):
             span = slice(j * unit, (j + 1) * unit)
@@ -418,9 +423,9 @@
             final = (mine[u, span] + brecv[l, u, j].astype(F32)).astype(BF16)
             strm[l, span, out_cols(c, u)] = final
             if last_layer:
-                piece = strm.at[l, span, out_cols(c, u)]
-                lasts[u, j] = message(("c_own" if j else "c_near", u), piece, piece, core_dev, "last")
-                write(u, j, c)
+                piece, place = strm.at[l, span, out_cols(c, u)], out.at[span, out_cols(c, u)]
+                message(("c", 0), piece, place, core_dev, "last")
+                pltpu.make_async_copy(piece, place, out_sem.at[0]).start()
             else:
                 wide = final.astype(F32)
                 nrm[l + 1, pl.ds(al(PAD + q * toks + j * unit, 32), unit), out_cols(c, u)] = (
@@ -429,28 +434,19 @@
                 folded = sum(square[:, k * lanes:(k + 1) * lanes] for k in range(chunk // lanes))
                 squares[span, :] = folded if u == 0 else squares[span, :] + folded
 
-        def write(u, j, h):
-            span = slice(j * unit, (j + 1) * unit)
-            pltpu.make_async_copy(strm.at[l, span, out_cols(h, u)], out.at[span, out_cols(h, u)],
-                                  out_sem.at[0]).start()
-
-        def finish(u, j):
-            lasts[u, j].wait_recv()
-            write(u, j, 1 - c)
-
         def lot(b, u):
             return nrm.at[l + 1, pl.ds(al(PAD + b * toks, 32), toks), out_cols(c, u)]
 
         def pass_chunk(kind, u, b, dev):
-            moves[kind, u] = message((kind, u), lot(b, u), lot(b, u), dev, kind[0])
+            moves[kind, u] = message((kind if kind[0] == "g" else "c", u), lot(b, u), lot(b, u), dev, kind[0])
 
         def gather(u):
             pass_chunk("g_near", u, q, near_dev)
-            pass_chunk("g_far", u, q, far_dev)
             pass_chunk("c_own", u, q, core_dev)
 
         def forward(u):
             moves["g_near", u].wait_recv()
+            pass_chunk("g_far", u, q, far_dev)
             pass_chunk("g_pass", u, near, far_dev)
             pass_chunk("c_near", u, near, core_dev)
 
@@ -465,15 +461,14 @@
         def gate_chunk(u):
             if u > 0:
                 consume(l + 1, 0, u)
-            for kind in ("c_own", "c_near", "c_far", "c_diag"):
-                moves[kind, u].wait_recv()
+            all_came(("c", u), nrm.at[l + 1, PAD:PAD + group, 0:chunk])
             gate_part(l + 1, u, plane_at(u), PAD, group, toks)
 
         def send_squares():
             lane_id = lax.broadcasted_iota(jnp.int32, (toks, lanes), 1)
             total = jnp.sum(squares[...], axis=1, keepdims=True)
             qsend[l] = jnp.transpose(jnp.where(lane_id == 0, total, 0.0))[0:2, :]
-            return [message(("square", k), qsend.at[l], qrecv.at[l, k], dev, "square")
+            return [message(("square", k > 0), qsend.at[l], qrecv.at[l, k], dev, "square")
                     for k, dev in enumerate(plane_devs)]
 
         def row_scale(whole):
@@ -490,6 +485,8 @@
             edge.rise()
 
         def gate_final(edge):
+            u = planes - 1
+            consume(l + 1, 0, u)
             edge.finish()
 
             @pl.when(z > 0)
@@ -501,51 +498,58 @@
 
             both = jnp.dot(nrm[l + 1, 0:PAD, :], wvg[l + 1], preferred_element_type=F32)
             gat[0:PAD, :] = (both[:, :ch] * jax.nn.sigmoid(both[:, ch:])).astype(BF16).astype(F32)
-            for m in norms[1:]:
-                m.wait_recv()
+            all_came(("square", True), qrecv.at[l, 1:])
+            all_came(("c", u), nrm.at[l + 1, PAD:PAD + group, 0:chunk])
+            depth = pl.ds(al(plane_at(u) * 4 * rows, 4 * rows), 4 * rows)
             for k in range(4):
                 mate = qsend[l] if k == 0 else qrecv[l, 2 * k - 1]
                 scale = row_scale(mate + qrecv[l, 2 * k])
                 at = pl.ds(al(PAD + quad[k] * toks, 32), toks)
-                value, gate = acc[at, :ch] * scale, acc[at, ch:] * scale
+                both = acc[at, :] + jnp.dot(nrm[l + 1, at, depth], wvg[l + 1, depth, :],
+                                            preferred_element_type=F32)
+                value, gate = both[:, :ch] * scale, both[:, ch:] * scale
                 gat[at, :] = (value * jax.nn.sigmoid(gate)).astype(BF16).astype(F32)
 
         swaps, firsts, seconds, lasts, moves = {}, {}, {}, {}, {}
-        lag = 4
-        for i in range(planes + lag + 1):
-            if i < planes:
-                stage_swap(i)
-            if 1 <= i <= planes:
-                stage_first(i - 1)
+        for u in range(planes - 1):
+            stage_swap(u)
+            if u > 0:
+                stage_first(u - 1)
+        stage_first(planes - 2)
+        stage_swap(planes - 1)
+        stage_first(planes - 1)
+        if last_layer:
+            drain(l, 0)
+            drain(l, 1)
+            pltpu.make_async_remote_copy(
+                wvg.at[:, 0:9 * rows // 2, :], wvg.at[:, 0:9 * rows // 2, :], wx_send.at[0],
+                wx_recv.at[0, 0], device_id=core_dev, device_id_type=MESH).wait_send()
+            all_sent("ag", nrm.at[0, PAD:PAD + 5 * toks // 2, :])
+            all_sent("sum", srecv)
+            if layers > 1:
+                all_sent("square", qrecv.at[0:layers - 1])
+                all_sent("g", nrm.at[1:layers, PAD:PAD + 3 * toks, 0:half])
+                all_sent("c", nrm.at[1:layers, PAD:PAD + group, 0:half])
+        for u in range(planes - 1):
             for j in range(2):
-                if 0 <= i - lag < planes:
-                    stage_second(i - lag, j)
-                if 0 <= i - lag - 1 < planes:
-                    stage_last(i - lag - 1, j)
+                stage_take(u, j)
+            if u + 2 == planes:
+                for uu in range(planes - 1):
+                    for j in range(2):
+                        stage_give(uu, j)
+        for j in range(2):
+            stage_take(planes - 1, j)
+            stage_give(planes - 1, j)
+        if not last_layer:
+            pump(l + 1, 0, 1)
+        for u in range(planes):
+            for j in range(2):
+                stage_last(u, j)
             if not last_layer:
-                if i - lag - 1 >= 0:
-                    gather(i - lag - 1)
-                if i - lag - 3 >= 0:
-                    forward(i - lag - 3)
-                if i == lag + 2:
-                    pump(l + 1, 0, 1)
-            if last_layer and i == planes:
-                drain(l, 0)
-                drain(l, 1)
-                pltpu.make_async_remote_copy(
-                    wvg.at[:, 0:9 * rows // 2, :], wvg.at[:, 0:9 * rows // 2, :], wx_send.at[0],
-                    wx_recv.at[0, 0], device_id=core_dev, device_id_type=MESH).wait_send()
-                all_sent("ag", nrm.at[0, PAD:PAD + 5 * toks // 2, :])
-                all_sent("sum", srecv)
-                if layers > 1:
-                    all_sent("square", qrecv.at[0:layers - 1])
-                    all_sent("g", nrm.at[1:layers, PAD:PAD + 3 * toks, 0:half])
-                    all_sent("c", nrm.at[1:layers, PAD:PAD + group, 0:half])
-        if last_layer:
-            for u in range(planes):
-                for j in range(2):
-                    finish(u, j)
-        else:
+                gather(u)
+                if u >= 2:
+                    forward(u - 2)
+        if not last_layer:
             edge = Halo(l + 1, edge_out.at[l], edge_in.at[l, c])
             norms = send_squares()
             cross_far(0)
@@ -564,7 +568,8 @@
                 if u == ahead + 1:
                     edge.spread()
                     pump(l + 1, 1, 0)
-                gate_chunk(u - ahead)
+                if u - ahead < planes - 1:
+                    gate_chunk(u - ahead)
                 if u == ahead + 2:
                     drain(l, 0)
                     drain(l, 1)
@@ -576,7 +581,9 @@
     all_sent("first", asend)
     all_sent("second", bsend)
     all_sent("last", strm.at[layers - 1, :, 0:half])
-    pltpu.make_async_copy(strm.at[layers - 1], out, out_sem.at[0]).wait()
+    whole_half = strm.at[layers - 1, :, 0:half]
+    pltpu.make_async_copy(whole_half, out.at[:, 0:half], out_sem.at[0]).wait()
+    all_came(("c", 0), whole_half)
 
 
 def fused(n, layers):
@@ -588,7 +595,7 @@
         chunk = 2 * rows
         taps = jnp.transpose(conv_taps, (1, 0, 2))
         hbm = pl.BlockSpec(memory_space=pltpu.HBM)
-        msgs = 7 + 7 * PARTS + 13 * planes
+        msgs = 2 + PARTS + 10 * planes
         return pl.pallas_call(
             functools.partial(kernel, n, layers, taps_n),
             out_shape=jax.ShapeDtypeStruct((toks, width), BF16),
@@ -605,8 +612,8 @@
                 pltpu.VMEM((PAD + group, ch), F32),
                 pltpu.VMEM((group, ch), F32),
                 pltpu.VMEM((group, ch), BF16),
-                pltpu.VMEM((layers, PARTS, 2, group // PARTS), F32),
-                pltpu.VMEM((layers, PARTS, 7, 2, group // PARTS), F32),
+                pltpu.VMEM((layers, 2, group), F32),
+                pltpu.VMEM((layers, 7, 2, group), F32),
                 pltpu.VMEM((layers, planes, 2, 2, toks, chunk), BF16),
                 pltpu.VMEM((layers, planes, 2, 2, toks, chunk), BF16),
                 pltpu.VMEM((layers, planes, 2, 2, toks // 2, chunk), BF16),

time: 133 us -> 128 us (0.962)
  Pallas kernels: 130 us -> 126 us
    pallas_call x1, Pallas kernels: 130 us -> 126 us  [body(): pl.pallas_call(functools.partial(kernel, n, layers, taps_n), out_shape=ja...]
where the time goes in v6:
time: 128 us
  Pallas kernels  126 us (98%)
  local copies, waits for them, and re-layouts  2.3 us (2%)
    pallas_call x1, Pallas kernels, body(): pl.pallas_call(functools.partial(kernel, n, layers, taps_n), out_shape=ja...  126 us

profile of v6, /device:TPU:0, one launch (start us, length us, event | category | flops | bytes accessed | tf_op | source)
XLA Modules:
  0.0 128.0 jit_solution(1099522423423431210)
XLA Ops:
  0.0 125.6 %shard_map.73 = bf16[256,2048]{1,0:T(8,128)(2,1)} custom-call(bf16[256,2048]{1,0:T(8,128)(2,1)} %stream_hbm.1, f32[2,2048]{1,0:T(2,128)} %gain_hbm.1, bf16[2,128,1024]{2,1,0:T(8,128)(2,1)} %vw.1, bf16[2,128,1024]{2,1,0:T(8,128)(2,1)} %gw.1, f32[31,2,1024]{2,1,0:T(2,128)} %bitcast.1, f32[2,1024]{1,0:T(2,128)} %cgain_hbm.1, bf16[2,1024,128]{2,1,0:T(8,128)(2,1)} %ow.1), custom_call_target="tpu_custom_call" | custom-call | tf_op jit(solution)/shard_map/pallas_call | solution.py:599
  125.6 2.3 %copy.9 = bf16[256,2048]{1,0:T(8,128)(2,1)} copy(bf16[256,2048]{1,0:T(8,128)(2,1)} %shard_map.73) | data formatting | bytes 2097152

commit v7 on v6

--- a/solution.py
+++ b/solution.py
@@ -13,6 +13,7 @@
 BF16 = jnp.bfloat16
 PAD = 32
 PARTS = 2
+EARLY = ((1, 0), (2, 0), (1, 1), (2, 1), (3, 0), (3, 1))
 
 
 def kernel(n, layers, taps_n, stream_hbm, gain_hbm, vw, gw, taps_hbm, cgain_hbm, ow, out,
@@ -93,10 +94,12 @@
     pl.semaphore_wait(barrier, len(plane_devs) + (z < planes - 1).astype(jnp.int32)
                       + (z > 0).astype(jnp.int32))
 
-    def z_copy(l, grp, d, t, hop, first, count, pair):
+    def z_copy(l, grp, d, t, hop, first, count, pair, kind=None):
         plane = z - t if d == 0 else z + t
         block = pl.ds(al((plane * 4 + first) * rows, rows), count * rows)
         ref = wvg.at[l, block, :] if grp == 0 else wo.at[l, :, block]
+        if kind is not None:
+            ref = wvg.at[l, block, kind * ch:(kind + 1) * ch]
         idx = (l * 2 + grp) * 2 + d
         return pltpu.make_async_remote_copy(
             ref, ref, z_send.at[idx, hop], z_recv.at[idx, hop, pair],
@@ -111,7 +114,15 @@
     def sends(d):
         return z < planes - 1 if d == 0 else z > 0
 
-    def pump(l, grp, t, ks=(0, 1, 2, 3)):
+    def pump_early():
+        for k, kind in EARLY:
+            shared[0, kind, k].wait_recv()
+            for d in range(2):
+                @pl.when(sends(d))
+                def _(k=k, d=d, kind=kind):
+                    z_copy(0, 0, d, 0, 0, quad[k], 1, k // 2, kind).start()
+
+    def pump(l, grp, t, ks=(0, 1, 2, 3), pairs=(0, 1)):
         if t == 0:
             for k in ks:
                 for kind in ((0, 1) if grp == 0 else (2,)):
@@ -125,7 +136,7 @@
                         def _(k=k, d=d):
                             z_copy(l, grp, d, 0, 0, quad[k], 1, k // 2).start()
         if t > 0 or l > 0:
-            for pair in range(2):
+            for pair in pairs:
                 for d in range(2):
                     @pl.when(holds(d, t) & sends(d))
                     def _(pair=pair, d=d):
@@ -171,7 +182,8 @@
         pltpu.make_async_remote_copy(ref, ref, msg_send.at[kinds_sent[sender]], msg_recv.at[0],
                                      device_id=core_dev, device_id_type=MESH).wait_send()
 
-    share(0, (0, 1))
+    for k, kind in EARLY:
+        shared_copy(0, kind, k)
 
     def block_rows(b):
         return pl.ds(al(b * toks, toks), toks)
@@ -292,7 +304,7 @@
             edge.rise()
             own_near = [message(("g_near", j), spot(q, j), spot(q, j), near_dev, ("near", j)) for j in range(2)]
             passed, relays, own_far = [], {}, []
-            pump(0, 0, 0, (1, 2, 3))
+            pump_early()
             edge.spread()
             to_far(0)
             to_far(1)
@@ -330,21 +342,22 @@
             pump(0, 1, 1)
 
         lead = PAD - (taps_n - 1)
-        step_rows = 64
+        step_rows = 128
 
         def conv_step(r, _):
             at = al(r * step_rows, step_rows)
             for lane in range(ch // lanes):
                 cut = slice(lane * lanes, (lane + 1) * lanes)
-                total = jnp.zeros((step_rows, lanes), F32)
+                total = [None, None]
                 block = gat[pl.ds(at, step_rows + PAD), cut]
                 for b in range(8):
                     moved = block if b == 0 else pltpu.roll(block, step_rows + PAD - b, 0)
                     for a in range(PAD // 8 + 1):
                         tap = 8 * a + b - lead
                         if 0 <= tap < taps_n:
-                            total = total + taps[tap, l:l + 1, cut] * moved[8 * a:8 * a + step_rows]
-                fil[pl.ds(at, step_rows), cut] = total
+                            term = taps[tap, l:l + 1, cut] * moved[8 * a:8 * a + step_rows]
+                            total[a % 2] = term if total[a % 2] is None else total[a % 2] + term
+                fil[pl.ds(at, step_rows), cut] = total[0] + total[1]
             return 0
 
         sums = []

time: 128 us -> 128 us (level)
  no operation moved by 1% of the time
where the time goes in v7:
time: 128 us
  Pallas kernels  125 us (98%)
  local copies, waits for them, and re-layouts  2.3 us (2%)
    pallas_call x1, Pallas kernels, body(): pl.pallas_call(functools.partial(kernel, n, layers, taps_n), out_shape=ja...  125 us

profile of v7, /device:TPU:0, one launch (start us, length us, event | category | flops | bytes accessed | tf_op | source)
XLA Modules:
  0.0 127.6 jit_solution(8099315223604224427)
XLA Ops:
  0.0 125.3 %shard_map.73 = bf16[256,2048]{1,0:T(8,128)(2,1)} custom-call(bf16[256,2048]{1,0:T(8,128)(2,1)} %stream_hbm.1, f32[2,2048]{1,0:T(2,128)} %gain_hbm.1, bf16[2,128,1024]{2,1,0:T(8,128)(2,1)} %vw.1, bf16[2,128,1024]{2,1,0:T(8,128)(2,1)} %gw.1, f32[31,2,1024]{2,1,0:T(2,128)} %bitcast.1, f32[2,1024]{1,0:T(2,128)} %cgain_hbm.1, bf16[2,1024,128]{2,1,0:T(8,128)(2,1)} %ow.1), custom_call_target="tpu_custom_call" | custom-call | tf_op jit(solution)/shard_map/pallas_call | solution.py:612
  125.3 2.3 %copy.9 = bf16[256,2048]{1,0:T(8,128)(2,1)} copy(bf16[256,2048]{1,0:T(8,128)(2,1)} %shard_map.73) | data formatting | bytes 2097152

commit v8 on v7

--- a/solution.py
+++ b/solution.py
@@ -78,7 +78,8 @@
             copy = pltpu.make_async_copy(src, dst, loc_sem.at[idx])
         else:
             copy = pltpu.make_async_remote_copy(
-                src, dst, wx_send.at[0], wx_recv.at[idx, k - 1],
+                src, dst, wx_send.at[0],
+                wx_recv.at[idx * 3 + k - 1 if l == 0 else 7 + 2 * l + kind // 2],
                 device_id=(z * 4 + quad[k], c), device_id_type=MESH)
         copy.start()
         shared[l, kind, k] = copy
@@ -126,15 +127,19 @@
         if t == 0:
             for k in ks:
                 for kind in ((0, 1) if grp == 0 else (2,)):
-                    if k:
+                    if k == 0:
+                        shared[l, kind, k].wait()
+                    elif l == 0:
                         shared[l, kind, k].wait_recv()
-                    else:
-                        shared[l, kind, k].wait()
                 if l == 0:
                     for d in range(2):
                         @pl.when(sends(d))
                         def _(k=k, d=d):
                             z_copy(l, grp, d, 0, 0, quad[k], 1, k // 2).start()
+        if t == 0 and l > 0:
+            three = wvg.at[l, 0:3 * rows, :] if grp == 0 else wo.at[l, :, 0:3 * rows]
+            pltpu.make_async_remote_copy(three, three, wx_send.at[0], wx_recv.at[7 + 2 * l + grp],
+                                         device_id=core_dev, device_id_type=MESH).wait_recv()
         if t > 0 or l > 0:
             for pair in pairs:
                 for d in range(2):
@@ -536,7 +541,7 @@
             drain(l, 1)
             pltpu.make_async_remote_copy(
                 wvg.at[:, 0:9 * rows // 2, :], wvg.at[:, 0:9 * rows // 2, :], wx_send.at[0],
-                wx_recv.at[0, 0], device_id=core_dev, device_id_type=MESH).wait_send()
+                wx_recv.at[0], device_id=core_dev, device_id_type=MESH).wait_send()
             all_sent("ag", nrm.at[0, PAD:PAD + 5 * toks // 2, :])
             all_sent("sum", srecv)
             if layers > 1:
@@ -647,7 +652,7 @@
                 pltpu.SemaphoreType.DMA((1,)),
                 pltpu.SemaphoreType.DMA((layers * 3,)),
                 pltpu.SemaphoreType.DMA((1,)),
-                pltpu.SemaphoreType.DMA((layers * 3, 3)),
+                pltpu.SemaphoreType.DMA((7 + 2 * layers,)),
                 pltpu.SemaphoreType.DMA((layers * 4, planes - 1)),
                 pltpu.SemaphoreType.DMA((layers * 4, planes - 1, 2)),
                 pltpu.SemaphoreType.DMA((layers, 5)),

time: 128 us -> 128 us (level)
  no operation moved by 1% of the time
where the time goes in v8:
time: 128 us
  Pallas kernels  125 us (98%)
  local copies, waits for them, and re-layouts  2.3 us (2%)
    pallas_call x1, Pallas kernels, body(): pl.pallas_call(functools.partial(kernel, n, layers, taps_n), out_shape=ja...  125 us

profile of v8, /device:TPU:0, one launch (start us, length us, event | category | flops | bytes accessed | tf_op | source)
XLA Modules:
  0.0 127.6 jit_solution(9128241172251710312)
XLA Ops:
  0.0 125.3 %shard_map.73 = bf16[256,2048]{1,0:T(8,128)(2,1)} custom-call(bf16[256,2048]{1,0:T(8,128)(2,1)} %stream_hbm.1, f32[2,2048]{1,0:T(2,128)} %gain_hbm.1, bf16[2,128,1024]{2,1,0:T(8,128)(2,1)} %vw.1, bf16[2,128,1024]{2,1,0:T(8,128)(2,1)} %gw.1, f32[31,2,1024]{2,1,0:T(2,128)} %bitcast.1, f32[2,1024]{1,0:T(2,128)} %cgain_hbm.1, bf16[2,1024,128]{2,1,0:T(8,128)(2,1)} %ow.1), custom_call_target="tpu_custom_call" | custom-call | tf_op jit(solution)/shard_map/pallas_call | solution.py:617
  125.3 2.3 %copy.9 = bf16[256,2048]{1,0:T(8,128)(2,1)} copy(bf16[256,2048]{1,0:T(8,128)(2,1)} %shard_map.73) | data formatting | bytes 2097152
